TPU v7x, 256 devices: a whole 4x4x8 slice. The times are simulated.
256 devices in a mesh: ep: 16 (over y, x), tp: 16 (over z, core).
Axes of the slice: x: 4, y: 4, z: 8, core: 2. Of those that a mesh axis runs over, the one named last changes fastest.
Arguments:
- query_latent: bfloat16 [8192, 1024], P('ep'), may hold values from -6 to 6
- joint_latent: bfloat16 [8192, 512], P('ep'), may hold values from -6 to 6
- rotary_key: bfloat16 [8192, 32], P('ep'), may hold values from -60 to 60
- query_gain: float32 [1024], replicated, may hold values from 0.1 to 1.9
- joint_gain: float32 [512], replicated, may hold values from 0.1 to 1.9
- query_weight: bfloat16 [1024, 2048], P(None, 'tp'), may hold values from -0.1875 to 0.1875
- query_rotary: bfloat16 [1024, 1024], P(None, 'tp'), may hold values from -0.1875 to 0.1875
- key_weight: bfloat16 [512, 2048], P(None, 'tp'), may hold values from -0.25 to 0.25
- value_weight: bfloat16 [512, 2048], P(None, 'tp'), may hold values from -0.25 to 0.25
- output_weight: bfloat16 [2048, 2048], P('tp'), may hold values from -6 to 6
- expert_input: bfloat16 [8192, 2048], P('ep'), may hold values from -6 to 6
- expert_gain: float32 [2048], replicated, may hold values from 0.1 to 1.9
- routes: int32 [8192, 2], P('ep'), may hold values from 0 to 31, all different within a row; in each aligned block of 512 rows (0 to 511, 512 to 1023, ...) at most 48 rows name the same one
- route_weight: float32 [8192, 2], P('ep'), may hold values from 0.2 to 1
- gate_weight: bfloat16 [32, 2048, 4096], P('ep', None, 'tp'), may hold values from -0.125 to 0.125
- up_weight: bfloat16 [32, 2048, 4096], P('ep', None, 'tp'), may hold values from -0.125 to 0.125
- down_weight: bfloat16 [32, 4096, 2048], P('ep', 'tp'), may hold values from -0.09375 to 0.09375
Outputs:
- mixer_out: bfloat16 [8192, 2048], P(('ep', 'tp'))
- expert_out: bfloat16 [8192, 2048], P('ep', 'tp')
Inputs may be any that keep to these rules, and one draw needn't show every extreme that they name: `routes`: A row names 2 different experts. Among the rows of one device (aligned blocks of 512 rows) no expert is named by more than 48 rows, a bound that some block reaches.
All inputs are finite; a program needn't handle non-finite values.
Results may differ from a plain program's by a relative error of at most 0.019.
The roundings to bfloat16 on the way count: a program that leaves them out, or rounds other values in their place, can miss the bound.
Values may be sent and summed in bfloat16 or wider, within the bound.
A program may use at most 128 MiB of HBM per device.

v0:
```python
import jax
import jax.numpy as jnp
from jax import lax
from jax.sharding import PartitionSpec as P

NOPE = 64
VDIM = 64


NORM_EPSILON = 1e-06
ROTARY_BASE = 10000.0


def sent_together(arrays, axis, dim, along):
    both = jnp.concatenate(arrays, axis=along)
    out, at, outs = (lax.all_gather(both, axis, axis=dim, tiled=True), 0, [])
    for a in arrays:
        outs.append(lax.slice_in_dim(out, at, at + a.shape[along], axis=along))
        at += a.shape[along]
    return tuple(outs)


def norm_rows(source, gain_vector):
    as_float = source.astype(jnp.float32)
    factor = lax.rsqrt(jnp.mean(as_float * as_float, axis=-1, keepdims=True) + NORM_EPSILON)
    return (as_float * factor * gain_vector).astype(jnp.bfloat16)


def rotate(source, positions):
    half_width = source.shape[-1] // 2
    frequencies = ROTARY_BASE ** (-jnp.arange(half_width, dtype=jnp.float32) / half_width)
    angles = positions[:, None] * frequencies[None, :]
    view_shape = (source.shape[0],) + (1,) * (source.ndim - 2) + (half_width,)
    cosine_table = jnp.cos(angles).reshape(view_shape)
    sine_table = jnp.sin(angles).reshape(view_shape)
    first_half = source[..., :half_width]
    second = source[..., half_width:]
    return jnp.concatenate(
        [
            first_half * cosine_table - second * sine_table,
            second * cosine_table + first_half * sine_table,
        ],
        axis=-1,
    )


def attend_block(
    carried, query_plain, query_turned, key_block, value_block, turned_block, score_scale
):
    row_top, row_total, mixed_values = carried
    scores = jnp.einsum("qhd,khd->qhk", query_plain, key_block, preferred_element_type=jnp.float32)
    scores = scores + jnp.einsum(
        "qhd,kd->qhk", query_turned, turned_block, preferred_element_type=jnp.float32
    )
    scores = scores * score_scale
    new_top = jnp.maximum(row_top, jnp.max(scores, axis=-1))
    factor = jnp.exp(row_top - new_top)
    expo = jnp.exp(scores - new_top[..., None])
    row_total = row_total * factor + jnp.sum(expo, axis=-1)
    mixed_values = mixed_values * factor[..., None] + jnp.einsum(
        "qhk,khd->qhd", expo.astype(jnp.bfloat16), value_block, preferred_element_type=jnp.float32
    )
    return (new_top, row_total, mixed_values)


def token_mixer(
    query_latent,
    joint_latent,
    rotary_key,
    query_gain,
    joint_gain,
    query_weight,
    query_rotary,
    key_weight,
    value_weight,
    output_weight,
):
    row_count = query_latent.shape[0]
    head_count = key_weight.shape[1] // NOPE
    turn_width = rotary_key.shape[1]
    offset = lax.axis_index("ep") * row_count
    positions = (offset + jnp.arange(row_count, dtype=jnp.int32)).astype(jnp.float32)
    query_normed = norm_rows(query_latent, query_gain)
    joint_normed = norm_rows(joint_latent, joint_gain)
    turned_key = rotate(rotary_key.astype(jnp.float32), positions).astype(jnp.bfloat16)
    query_plain = jnp.dot(query_normed, query_weight, preferred_element_type=jnp.float32).astype(
        jnp.bfloat16
    )
    query_plain = query_plain.reshape(row_count, head_count, NOPE)
    query_turned = jnp.dot(query_normed, query_rotary, preferred_element_type=jnp.float32)
    query_turned = rotate(
        query_turned.reshape(row_count, head_count, turn_width), positions
    ).astype(jnp.bfloat16)
    score_scale = (NOPE + turn_width) ** (-0.5)
    start_carry = (
        jnp.full((row_count, head_count), -jnp.inf, jnp.float32),
        jnp.zeros((row_count, head_count), jnp.float32),
        jnp.zeros((row_count, head_count, VDIM), jnp.float32),
    )
    carried = start_carry
    latent_piece, turned_piece = sent_together((joint_normed, turned_key), "ep", 0, 1)
    block_rows = min(row_count, latent_piece.shape[0])
    block_total = latent_piece.shape[0] // block_rows

    def scan_step(inner_carry, key_items):
        latent_block, turned_block = key_items
        key_block = jnp.dot(latent_block, key_weight, preferred_element_type=jnp.float32)
        key_block = key_block.astype(jnp.bfloat16).reshape(block_rows, head_count, NOPE)
        value_block = jnp.dot(latent_block, value_weight, preferred_element_type=jnp.float32)
        value_block = value_block.astype(jnp.bfloat16).reshape(block_rows, head_count, VDIM)
        return (
            attend_block(
                inner_carry,
                query_plain,
                query_turned,
                key_block,
                value_block,
                turned_block,
                score_scale,
            ),
            None,
        )

    carried, _ = lax.scan(
        scan_step,
        carried,
        (
            latent_piece.reshape(block_total, block_rows, latent_piece.shape[1]),
            turned_piece.reshape(block_total, block_rows, turn_width),
        ),
    )
    row_top, row_total, mixed_values = carried
    attended = (
        (mixed_values / row_total[..., None])
        .astype(jnp.bfloat16)
        .reshape(row_count, head_count * VDIM)
    )
    return lax.psum_scatter(
        jnp.dot(attended, output_weight, preferred_element_type=jnp.float32).astype(jnp.bfloat16),
        "tp",
        scatter_dimension=0,
        tiled=True,
    )


def experts(expert_input, expert_gain, routes, route_weight, gate_weight, up_weight, down_weight):
    row_count = expert_input.shape[0]
    feature_width = expert_input.shape[1]
    top_count = routes.shape[1]
    group_count = lax.axis_size("ep")
    local_count = gate_weight.shape[0]
    expert_count = local_count * group_count
    capacity = 3 * row_count // (2 * group_count)
    part_width = feature_width // lax.axis_size("tp")
    flat_routes = routes.reshape(-1)
    onehot = (flat_routes[:, None] == jnp.arange(expert_count, dtype=jnp.int32)[None, :]).astype(
        jnp.int32
    )
    rank_within = jnp.sum((jnp.cumsum(onehot, axis=0) - onehot) * onehot, axis=1)
    slot_index = flat_routes * capacity + rank_within
    owner_token = jnp.arange(row_count * top_count, dtype=jnp.int32) // top_count
    slot_token = jnp.zeros((expert_count * capacity,), jnp.int32).at[slot_index].set(owner_token)
    filled = jnp.zeros((expert_count * capacity,), jnp.bfloat16).at[slot_index].set(1.0)
    normed = norm_rows(expert_input, expert_gain)
    columns = lax.dynamic_slice_in_dim(normed, lax.axis_index("tp") * part_width, part_width, 1)
    outgoing = (columns[slot_token] * filled[:, None]).reshape(
        group_count, local_count, capacity, part_width
    )
    arrived = lax.all_to_all(outgoing, "ep", split_axis=0, concat_axis=0, tiled=True)
    piece = lax.all_gather(arrived, "tp", axis=3, tiled=True)
    gate_running = jnp.einsum(
        "secd,edf->secf", piece, gate_weight, preferred_element_type=jnp.float32
    )
    up_running = jnp.einsum("secd,edf->secf", piece, up_weight, preferred_element_type=jnp.float32)
    hidden = (jax.nn.silu(gate_running) * up_running).astype(jnp.bfloat16)
    partial_value = jnp.einsum(
        "secf,efd->secd", hidden, down_weight, preferred_element_type=jnp.float32
    )
    summed = lax.psum_scatter(
        partial_value.astype(jnp.bfloat16), "tp", scatter_dimension=3, tiled=True
    )
    returned = lax.all_to_all(summed, "ep", split_axis=0, concat_axis=0, tiled=True)
    picked = returned.reshape(expert_count * capacity, part_width)[slot_index]
    picked = picked.astype(jnp.float32).reshape(row_count, top_count, part_width)
    return jnp.sum(picked * route_weight[:, :, None], axis=1).astype(jnp.bfloat16)


def local(
    query_latent,
    joint_latent,
    rotary_key,
    query_gain,
    joint_gain,
    query_weight,
    query_rotary,
    key_weight,
    value_weight,
    output_weight,
    expert_input,
    expert_gain,
    routes,
    route_weight,
    gate_weight,
    up_weight,
    down_weight,
):
    mixer_out = token_mixer(
        query_latent,
        joint_latent,
        rotary_key,
        query_gain,
        joint_gain,
        query_weight,
        query_rotary,
        key_weight,
        value_weight,
        output_weight,
    )
    expert_out = experts(
        expert_input, expert_gain, routes, route_weight, gate_weight, up_weight, down_weight
    )
    return (mixer_out, expert_out)


def solution(mesh):
    return jax.shard_map(
        local,
        mesh=mesh,
        in_specs=(
            P("ep", None),
            P("ep", None),
            P("ep", None),
            P(),
            P(),
            P(None, "tp"),
            P(None, "tp"),
            P(None, "tp"),
            P(None, "tp"),
            P("tp", None),
            P("ep", None),
            P(),
            P("ep", None),
            P("ep", None),
            P("ep", None, "tp"),
            P("ep", None, "tp"),
            P("ep", "tp", None),
        ),
        out_specs=(P(("ep", "tp"), None), P("ep", "tp")),
        check_vma=False,
    )
```

profile of v0, /device:TPU:1, one launch (start us, length us, event | category | flops | bytes accessed | tf_op | source)
XLA Modules:
  0.0 351.4 jit_solution(10818710300028206992)
XLA Ops:
  7.2 4.2 %convert_element_type.83 = f32[512,2048]{1,0:T(8,128)} convert(bf16[512,2048]{1,0:T(8,128)(2,1)} %param.29) | non-fusion elementwise | flops 1048576 | bytes 6291456 | tf_op jit(solution)/shard_map/convert_element_type | solution.py:24
  12.7 9.0 %reduce-window.6 = s32[32,8,128]{2,1,0:T(8,128)S(1)} reduce-window(s32[32,8,128]{2,1,0:T(8,128)S(1)} %fusion.46, s32[]{:T(128)} %constant.30.clone.1), window={size=1x1x128 pad=0_0x0_0x127_0}, to_apply=%region_8.9 | reduce-window | flops 4161536 | bytes 262148 | tf_op jit(solution)/shard_map/reduce-window
  22.6 4.3 %scatter_custom_fusion = s32[1536]{0:T(1024)S(1)} fusion(s32[1024]{0:T(1024)S(1)} %bitcast.150, s32[1024]{0:T(1024)S(1)} %add_select_fusion, s32[]{:T(128)} %constant.30.clone.1), kind=kCustom, calls=%fused_computation.89 | custom fusion | bytes 6148 | tf_op jit(solution)/shard_map/scatter | solution.py:162
  26.9 7.6 %scatter_custom_fusion.1 = bf16[1536]{0:T(1024)(128)(2,1)S(1)} fusion(s32[1024]{0:T(1024)S(1)} %bitcast.151, bf16[1024]{0:T(1024)(128)(2,1)S(1)} %broadcast.163, bf16[]{:T(256)} %constant.82.clone.1), kind=kCustom, calls=%fused_computation.93 | custom fusion | bytes 3074 | tf_op jit(solution)/shard_map/scatter | solution.py:163
  36.5 3.2 gather_fusion
  40.0 16.6 %all_to_all.10 = bf16[16,2,48,128]{3,2,1,0:T(8,128)(2,1)S(1)} all-to-all(bf16[16,2,48,128]{3,2,1,0:T(8,128)(2,1)S(1)} %broadcast_multiply_fusion), channel_id=1, replica_groups=mesh['ep'=16,'tp'=16] {'ep'}, dimensions={0} | all-to-all | bytes 786432 | tf_op jit(solution)/shard_map/all_to_all | solution.py:169
  59.7 1.9 pad_maximum_fusion
  64.4 50.7 %all-gather.5.cloned.1.call-done = bf16[16,2,48,2048]{3,2,0,1:T(8,128)(2,1)} async-done(((bf16[16,2,48,128]{3,2,0,1:T(8,128)(2,1)}), bf16[16,2,48,2048]{3,2,0,1:T(8,128)(2,1)}) %all-gather.5.cloned.1.call-update) | async-done | bytes 6291472 | tf_op jit(solution)/shard_map/all_gather | solution.py:170
  115.1 6.3 %fusion.23 = f32[2,16,48,256]{3,2,1,0:T(8,128)} fusion(bf16[16,2,48,2048]{3,2,0,1:T(8,128)(2,1)} %all-gather.5.cloned.1.call-done, bf16[2,2048,256]{2,1,0:T(8,128)(2,1)} %param.33), kind=kOutput, calls=%fused_computation.40 | convolution fusion | flops 1610612736 | bytes 9961472 | tf_op jit(solution)/shard_map/secd,edf->secf/dot_general | solution.py:171
  121.4 10.0 %convert_bitcast_fusion = bf16[16,2,48,2048]{3,2,0,1:T(8,128)(2,1)} fusion(bf16[2,256,2048]{2,1,0:T(8,128)(2,1)S(1)} %copy-done, f32[2,16,48,256]{3,2,1,0:T(8,128)} %fusion.23, bf16[16,2,48,2048]{3,2,0,1:T(8,128)(2,1)} %all-gather.5.cloned.1.call-done, bf16[2,2048,256]{2,1,0:T(8,128)(2,1)} %param.34), kind=kOutput, calls=%fused_computation.29 | convolution fusion | flops 3226730496 | bytes 18350080 | tf_op jit(solution)/shard_map/secf,efd->secd/dot_general | solution.py:176
  131.4 23.1 %copy.56 = bf16[16,2,48,2048]{2,0,1,3:T(8,128)(2,1)} copy(bf16[16,2,48,2048]{3,2,0,1:T(8,128)(2,1)} %convert_bitcast_fusion) | data formatting | bytes 12582912
  154.5 29.7 %reshape.224 = bf16[2048,1536]{1,0:T(8,128)(2,1)} reshape(bf16[2048,2,16,48]{3,2,1,0:T(8,128)(2,1)} %bitcast.135) | data formatting | bytes 12582912
  184.5 17.0 %all-gather.3.cloned.1.call-done = bf16[8192,544]{1,0:T(8,128)(2,1)} async-done(((bf16[512,544]{1,0:T(8,128)(2,1)}), bf16[8192,544]{1,0:T(8,128)(2,1)}) %all-gather.3.cloned.1.call-update) | async-done | bytes 8912912 | tf_op jit(solution)/shard_map/all_gather | solution.py:16
  201.5 1.6 slice-done
  204.0 7.2 %slice.38 = bf16[8192,512]{1,0:T(8,128)(2,1)} slice(bf16[8192,544]{1,0:T(8,128)(2,1)} %all-gather.3.cloned.1.call-done), slice={[0:8192], [0:512]} | slice | bytes 16777216 | tf_op jit(solution)/shard_map/slice | solution.py:18
  211.1 73.0 %while.15 = (s32[]{:T(128)}, f32[512,2]{0,1:T(2,128)S(1)}, f32[512,2]{0,1:T(2,128)S(1)}, f32[512,2,64]{0,2,1:T(8,128)S(1)}, bf16[16,512,512]{2,1,0:T(8,128)(2,1)...) while((s32[]{:T(128)}, f32[512,2]{0,1:T(2,128)S(1)}, ...), condition=%wide.region_5.6_spmd.clone, body=%wide.region_2.5_spmd.clone.sunk | while | flops 305992704 | bytes 13141125 | solution.py:124
  284.2 3.1 convolution_convert_fusion.2
  287.4 2.1 reshape.225
  289.5 1.8 copy.48
  291.3 5.0 %all-to-all-start.1 = ((bf16[16,2,48,128]{3,2,1,0:T(8,128)(2,1)}), bf16[16,2,48,128]{3,2,1,0:T(8,128)(2,1)S(1)}, u32[]{:S(2)}, u32[]{:S(2)}) async-start(bf16[16,2,48,128]{3,2,1,0:T(8,128)(2,1)} %copy.48), calls=%async_computation.2 | async-start | bytes 786432 | tf_op jit(solution)/shard_map/all_to_all | solution.py:182
  296.4 8.9 %all-to-all-done.1 = bf16[16,2,48,128]{3,2,1,0:T(8,128)(2,1)S(1)} async-done(((bf16[16,2,48,128]{3,2,1,0:T(8,128)(2,1)}), bf16[16,2,48,128]{3,2,1,0:T(8,128)(2,1)S(1)}, u32[]{:S(2)}, u32[]{:S(2)}) %all-to-all-start.1) | async-done | bytes 393248 | tf_op jit(solution)/shard_map/all_to_all | solution.py:182
  305.3 3.2 gather_fusion.1
  308.5 3.5 fusion.37
  311.9 32.9 %reduce-scatter.5.cloned.1.call-done = bf16[32,2048]{1,0:T(8,128)(2,1)} async-done(((bf16[512,2048]{1,0:T(8,128)(2,1)}), bf16[32,2048]{1,0:T(8,128)(2,1)}) %reduce-scatter.5.cloned.1.call-update) | async-done | bytes 131088 | tf_op jit(solution)/shard_map/reduce_scatter | solution.py:138
  (234 shorter events, 83.0 us)
Async XLA Ops:
  7.2 114.3 %copy-start = (bf16[2,256,2048]{2,1,0:T(8,128)(2,1)S(1)}, bf16[2,256,2048]{2,1,0:T(8,128)(2,1)}, u32[]{:S(2)}) copy-start(bf16[2,256,2048]{2,1,0:T(8,128)(2,1)} %param.35) | copy-start | bytes 6291460
  7.2 107.9 %all-gather.5.cloned.1.call-start = ((), (), s32[]{:S(2)}) async-start(), calls=%async_computation.6 | async-start | bytes 6684672 | tf_op jit(solution)/shard_map/all_gather | solution.py:170
  7.2 4.2 %copy-start.2 = (bf16[512,2048]{1,0:T(8,128)(2,1)S(1)}, bf16[512,2048]{1,0:T(8,128)(2,1)}, u32[]{:S(2)}) copy-start(bf16[512,2048]{1,0:T(8,128)(2,1)} %param.29) | copy-start | bytes 6291460
  11.4 0.7 copy-start.11
  39.7 17.8 %copy-start.10 = (bf16[512,32]{0,1:T(8,128)(2,1)S(1)}, bf16[512,32]{0,1:T(8,128)(2,1)}, u32[]{:S(2)}) copy-start(bf16[512,32]{0,1:T(8,128)(2,1)} %param.21) | copy-start | bytes 98308
  39.7 19.6 %copy-start.5 = (bf16[512,512]{1,0:T(8,128)(2,1)S(1)}, bf16[512,512]{1,0:T(8,128)(2,1)}, u32[]{:S(2)}) copy-start(bf16[512,512]{1,0:T(8,128)(2,1)} %param.20) | copy-start | bytes 1572868
  39.7 19.7 %copy-start.13 = (f32[512]{0:T(512)S(1)}, f32[512]{0:T(512)}, u32[]{:S(2)}) copy-start(f32[512]{0:T(512)} %param.23) | copy-start | bytes 6148
  57.4 144.1 %all-gather.3.cloned.1.call-start = ((), (), s32[]{:S(2)}) async-start(), calls=%async_computation.4 | async-start | bytes 11141120 | tf_op jit(solution)/shard_map/all_gather | solution.py:16
  59.4 2.8 copy-start.15
  59.6 2.3 copy-start.6
  61.6 2.1 copy-start.8
  61.6 2.1 copy-start.9
  61.6 225.7 %reduce-scatter.7.cloned.1.call-start = ((), (), s32[]{:S(2)}) async-start(), calls=%async_computation.7 | async-start | bytes 6684672
  61.9 1.9 copy-start.7
  61.9 1.9 copy-start.14
  184.2 160.6 %reduce-scatter.5.cloned.1.call-start = ((), (), s32[]{:S(2)}) async-start(), calls=%async_computation.5 | async-start | bytes 2228224 | tf_op jit(solution)/shard_map/reduce_scatter | solution.py:138
  201.5 1.6 slice-start
  203.9 7.2 %copy-start.3 = (bf16[512,128]{1,0:T(8,128)(2,1)S(1)}, bf16[512,128]{1,0:T(8,128)(2,1)}, u32[]{:S(2)}) copy-start(bf16[512,128]{1,0:T(8,128)(2,1)} %param.26) | copy-start | bytes 393220
  203.9 7.2 %copy-start.4 = (bf16[512,128]{1,0:T(8,128)(2,1)S(1)}, bf16[512,128]{1,0:T(8,128)(2,1)}, u32[]{:S(2)}) copy-start(bf16[512,128]{1,0:T(8,128)(2,1)} %param.27) | copy-start | bytes 393220
  287.3 8.9 %copy-start.12 = (f32[512,2]{0,1:T(2,128)S(1)}, f32[512,2]{0,1:T(2,128)}, u32[]{:S(2)}) copy-start(f32[512,2]{0,1:T(2,128)} %param.32) | copy-start | bytes 12292
  289.5 55.4 %copy-start.1 = (bf16[2,256,2048]{2,1,0:T(8,128)(2,1)S(1)}, bf16[2,256,2048]{2,1,0:T(8,128)(2,1)}, u32[]{:S(2)}) copy-start(bf16[2,256,2048]{2,1,0:T(8,128)(2,1)} %param.35) | copy-start | bytes 6291460
  291.3 14.0 %all-to-all-start.1 = ((bf16[16,2,48,128]{3,2,1,0:T(8,128)(2,1)}), bf16[16,2,48,128]{3,2,1,0:T(8,128)(2,1)S(1)}, u32[]{:S(2)}, u32[]{:S(2)}) async-start(bf16[16,2,48,128]{3,2,1,0:T(8,128)(2,1)} %copy.48), calls=%async_computation.2 | async-start | bytes 786432 | tf_op jit(solution)/shard_map/all_to_all | solution.py:182
Sparse Core Ops, SparseCore 0:
  57.5 57.5 all-gather.4
  117.5 83.9 all-gather.2
  204.1 63.9 reduce-scatter.6
  287.4 57.3 reduce-scatter.4
where the time goes:
time: 356 us; the launch traced here: 351 us
  waiting for transfers between devices  110 us (31%)
  local copies, waits for them, and re-layouts  88.7 us (25%)
  matrix products  88 us (25%)
  other arithmetic  27.5 us (8%)
  blocking collectives  16.6 us (5%)
  between operations  14.3 us (4%)
  starting transfers between devices  5.52 us (2%)
    unnamed x38, local copies, waits for them, and re-layouts  56.3 us
    all_gather x1, waiting for transfers between devices, experts(): piece = lax.all_gather(arrived, 'tp', axis=3, tiled=True)  50.7 us
    reduce_scatter x1, waiting for transfers between devices, token_mixer(): lax.psum_scatter(jnp.dot(attended, output_weight, preferred_element_type=...  32.9 us
    dot_general x16, matrix products, scan_step(): jnp.dot(latent_block, value_weight, preferred_element_type=jnp.float32)  21.7 us
    dot_general x16, matrix products, scan_step(): jnp.dot(latent_block, key_weight, preferred_element_type=jnp.float32)  21.7 us
    all_gather x1, waiting for transfers between devices, sent_together(): out, at, outs = (lax.all_gather(both, axis, axis=dim, tiled=True), 0, [])  17 us
    all_to_all x1, blocking collectives, experts(): lax.all_to_all(outgoing, 'ep', split_axis=0, concat_axis=0, tiled=True)  16.6 us
    dot_general x1, matrix products, experts(): jnp.einsum('secf,efd->secd', hidden, down_weight, preferred_element_type=...  10 us
  transfers between devices with their start and end apart: 5, of which 4 were waited for; matrix products, arithmetic and copies ran while one was open for 48% of the time, Pallas kernels for 0%

commit v1 on v0

v1 whole, which is shorter than its diff:
```python
import functools

import jax
import jax.numpy as jnp
from jax import lax
from jax.experimental import pallas as pl
from jax.experimental.pallas import tpu as pltpu
from jax.sharding import PartitionSpec as P

NOPE = 64
VDIM = 64
ROPE = 32
NORM_EPSILON = 1e-06
ROTARY_BASE = 10000.0
LANES = 128
LOG2E = 1.4426950408889634
MESH = pl.DeviceIdType.MESH
F32 = jnp.float32
BF16 = jnp.bfloat16


def ep_grid(count):
    return {16: (4, 4), 4: (2, 2), 2: (1, 2)}[count]


def dot(a, b):
    return jnp.dot(a, b, preferred_element_type=F32)


def dot_nt(a, b):
    return lax.dot_general(a, b, (((1,), (1,)), ((), ())), preferred_element_type=F32)


def front_kernel(
    cap, experts, ql, jl, rk_t, qgain, jgain, wa, wb, cq, sq, wk_t, wv, xin, egain, routes, routes_t,
    slots_out, kt_out, v_out, q_out, slot_out,
):
    tokens = ql.shape[0]
    half = tokens // 2

    def normed(ref, gain):
        x = ref[...].astype(F32)
        factor = lax.rsqrt(jnp.mean(x * x, axis=-1, keepdims=True) + NORM_EPSILON)
        return (x * factor * gain[...]).astype(BF16)

    r = routes[...]
    rt = routes_t[...]
    row = lax.broadcasted_iota(jnp.int32, (tokens, tokens), 0)
    col = lax.broadcasted_iota(jnp.int32, (tokens, tokens), 1)
    lane_e = lax.broadcasted_iota(jnp.int32, (tokens, experts), 1)
    named0 = lane_e == r[:, 0:1]
    named1 = lane_e == r[:, 1:2]
    named = (named0 | named1).astype(F32).astype(BF16)
    before = dot((col < row).astype(F32).astype(BF16), named)
    place = before.astype(jnp.int32) + lane_e * cap
    slot0 = jnp.sum(jnp.where(named0, place, 0), axis=1, keepdims=True)
    slot1 = jnp.sum(jnp.where(named1, place, 0), axis=1, keepdims=True)
    slot_out[...] = jnp.concatenate([slot0, slot1], axis=1)

    sub_e = lax.broadcasted_iota(jnp.int32, (experts, tokens), 0)
    named_t = (sub_e == rt[0:1, :]) | (sub_e == rt[1:2, :])
    before_t = dot(named_t.astype(F32).astype(BF16), (row < col).astype(F32).astype(BF16))
    rank_t = jnp.where(named_t, before_t, -1.0)

    x = xin[...].astype(F32)
    factor = lax.rsqrt(jnp.mean(x * x, axis=-1, keepdims=True) + NORM_EPSILON)
    at = pl.multiple_of(lax.axis_index("tp") * LANES, LANES)
    mine = (xin[:, pl.ds(at, LANES)].astype(F32) * factor * egain[:, pl.ds(at, LANES)]).astype(BF16)
    place_in = lax.broadcasted_iota(jnp.int32, (cap, tokens), 0).astype(F32)
    for e in range(experts):
        pick = (place_in == rank_t[e : e + 1, :]).astype(F32).astype(BF16)
        slots_out[e] = dot(pick, mine).astype(BF16)

    jn = normed(jl, jgain)
    kt = dot_nt(wk_t[...], jn).astype(BF16)
    rkt = rk_t[...]
    vv = dot(jn, wv[...]).astype(BF16)
    for h in range(2):
        part = slice(h * half, (h + 1) * half)
        kt_out[h, 0:NOPE, :] = kt[0:NOPE, part]
        kt_out[h, NOPE : NOPE + ROPE, :] = rkt[:, part]
        kt_out[h, NOPE + ROPE :, :] = kt[NOPE:, part]
        v_out[h] = vv[part]

    qn = normed(ql, qgain)
    q_out[...] = (dot(qn, wa[...]) * cq[...] + dot(qn, wb[...]) * sq[...]).astype(BF16)


def main_kernel(
    dims, slots, kt_own, v_own, q_ref, slot_ref, rw_ref, wg_hbm, wu_hbm, wd_hbm, wo_ref,
    mixer_ref, expert_ref,
    xbuf, pbuf, sbuf, rbuf, tbuf, fin, ret, ktb, vb, wg, wu, wd, m_s, l_s, acc_s,
    ap, asb, arb, atb,
    a2a_s, a2a_r, zs, zr, dds, ddr, kvs, kvr, pss, psr, rss, rsr, bks, bkr, aps, apr, ars, arr, local_s,
):
    ny, nx, nz, cap = dims
    ep_n = ny * nx
    rows = ep_n * cap
    ep = lax.axis_index("ep")
    tp = lax.axis_index("tp")
    y, x = ep // nx, lax.rem(ep, nx)
    z, c = tp // 2, lax.rem(tp, 2)
    oc = 1 - c
    sib = z * 2 + oc
    zright = lax.rem(z + 1, nz)
    zleft = lax.rem(z + nz - 1, nz)
    pending = []

    def send(src, dst, ssem, rsem, to):
        d = pltpu.make_async_remote_copy(
            src_ref=src, dst_ref=dst, send_sem=ssem, recv_sem=rsem, device_id=to, device_id_type=MESH
        )
        d.start()
        pending.append(d)

    def arrived(dst, ssem, rsem, frm):
        pltpu.make_async_remote_copy(
            src_ref=dst, dst_ref=dst, send_sem=ssem, recv_sem=rsem, device_id=frm, device_id_type=MESH
        ).wait_recv()

    own = [
        pltpu.make_async_copy(wg_hbm, wg, local_s.at[0]),
        pltpu.make_async_copy(wu_hbm, wu, local_s.at[1]),
        pltpu.make_async_copy(wd_hbm, wd, local_s.at[2]),
        pltpu.make_async_copy(slots.at[ep], xbuf.at[:, z, c, pl.ds(pl.multiple_of(ep * cap, 16), cap)], local_s.at[3]),
        pltpu.make_async_copy(kt_own.at[0], ktb.at[0, y, x], local_s.at[4]),
        pltpu.make_async_copy(kt_own.at[1], ktb.at[1, x, y], local_s.at[5]),
        pltpu.make_async_copy(v_own.at[0], vb.at[0, y, x], local_s.at[6]),
        pltpu.make_async_copy(v_own.at[1], vb.at[1, x, y], local_s.at[7]),
    ]
    for d in own[3:] + own[:3]:
        d.start()

    barrier = pltpu.get_barrier_semaphore()
    peers = [(lax.rem(ep + k, ep_n), tp) for k in range(1, ep_n)]
    peers.append((ep, sib))
    peers.append((ep, zright * 2 + c))
    if nz > 2:
        peers.append((ep, zleft * 2 + c))
    for peer in peers:
        pl.semaphore_signal(barrier, inc=1, device_id=peer, device_id_type=MESH)
    pl.semaphore_wait(barrier, len(peers))

    mine = pl.ds(pl.multiple_of(ep * cap, 16), cap)
    for k in range(1, ep_n):
        to = lax.rem(ep + k, ep_n)
        send(slots.at[to], xbuf.at[:, z, c, mine], a2a_s.at[k], a2a_r.at[k], (to, tp))

    axes = (("x", nx, x), ("y", ny, y))

    def ring_to(name, step):
        if name == "x":
            return (y * nx + lax.rem(x + nx + step, nx), tp)
        return (lax.rem(y + ny + step, ny) * nx + x, tp)

    def kv_refs(part, phase, block):
        other = (y, x)[part]
        if phase == 0:
            return ktb.at[part, other, block], vb.at[part, other, block]
        return ktb.at[part, block], vb.at[part, block]

    def kv_send(part, phase, step):
        name, n, me = axes[(part + phase) % 2]
        if n == 1 or step > n // 2:
            return
        tie = 2 * step == n
        for d, sign in ((0, 1), (1, -1)):
            block = lax.rem(me + n - sign * (step - 1), n)
            refs = kv_refs(part, phase, block)
            for kind in (0, 1):
                if not tie or kind == d:
                    i = (part, phase, d, step - 1, kind)
                    send(refs[kind], refs[kind], kvs.at[i], kvr.at[i], ring_to(name, sign))

    def kv_wait(part, phase, step):
        name, n, me = axes[(part + phase) % 2]
        if n == 1 or step > n // 2:
            return
        tie = 2 * step == n
        for d, sign in ((0, 1), (1, -1)):
            block = lax.rem(me + n - sign * step, n)
            refs = kv_refs(part, phase, block)
            for kind in (0, 1):
                if not tie or kind == d:
                    i = (part, phase, d, step - 1, kind)
                    arrived(refs[kind], kvs.at[i], kvr.at[i], ring_to(name, -sign))

    for i in (4, 5, 6, 7):
        own[i].wait()
    for part in (0, 1):
        kv_send(part, 0, 1)

    own[3].wait()
    for k in range(1, ep_n):
        frm = lax.rem(ep + ep_n - k, ep_n)
        there = xbuf.at[:, z, c, pl.ds(pl.multiple_of(frm * cap, 16), cap)]
        arrived(there, a2a_s.at[k], a2a_r.at[k], (frm, tp))

    hz = nz // 2
    hr = rows // 2
    z_to = ((ep, zright * 2 + c), (ep, zleft * 2 + c))

    def z_piece(e, block, core, d, step):
        if 2 * step == nz:
            return xbuf.at[e, block, core, pl.ds(d * hr, hr)]
        return xbuf.at[e, block, core]

    def z_send(e, step):
        for d, sign in ((0, 1), (1, -1)):
            block = lax.rem(z + nz - sign * (step - 1), nz)
            piece = z_piece(e, block, c, d, step)
            send(piece, piece, zs.at[e, d, step - 1], zr.at[e, d, step - 1], z_to[d])

    def z_wait(e, step):
        for d, sign in ((0, 1), (1, -1)):
            block = lax.rem(z + nz - sign * step, nz)
            piece = z_piece(e, block, c, d, step)
            arrived(piece, zs.at[e, d, step - 1], zr.at[e, d, step - 1], z_to[1 - d])
            if step < hz:
                after = lax.rem(z + nz - sign * step, nz)
                nxt = z_piece(e, after, c, d, step + 1)
                send(nxt, nxt, zs.at[e, d, step], zr.at[e, d, step], z_to[d])
            send(piece, piece, dds.at[e, d, step], ddr.at[e, d, step], (ep, sib))

    def dd_wait(e):
        there = xbuf.at[e, z, oc]
        arrived(there, dds.at[e, 0, 0], ddr.at[e, 0, 0], (ep, sib))
        for step in range(1, hz + 1):
            for d, sign in ((0, 1), (1, -1)):
                block = lax.rem(z + nz - sign * step, nz)
                piece = z_piece(e, block, oc, d, step)
                arrived(piece, dds.at[e, d, step], ddr.at[e, d, step], (ep, sib))

    for e in (0, 1):
        z_send(e, 1)
        piece = xbuf.at[e, z, c]
        send(piece, piece, dds.at[e, 0, 0], ddr.at[e, 0, 0], (ep, sib))

    scale = LOG2E * (NOPE + ROPE) ** (-0.5)
    tokens = q_ref.shape[0]
    q_tile = min(256, tokens)
    m_s[...] = jnp.full(m_s.shape, -jnp.inf, F32)
    l_s[...] = jnp.zeros(l_s.shape, F32)
    acc_s[...] = jnp.zeros(acc_s.shape, F32)

    def unit(part, a):
        blocks = (nx, ny)[part]

        def tile(t, carry):
            at = pl.ds(pl.multiple_of(t * q_tile, q_tile), q_tile)
            for head in (0, 1):
                q = q_ref[at, head * LANES : (head + 1) * LANES]
                s = jnp.concatenate(
                    [dot(q, ktb[part, a, b, head * ROPE : head * ROPE + LANES, :]) for b in range(blocks)], axis=1
                )
                m_old = m_s[head, at]
                m_new = jnp.maximum(m_old, jnp.max(s, axis=1, keepdims=True))
                alpha = jnp.exp2((m_old - m_new) * scale)
                p = jnp.exp2(s * scale - m_new[:, 0:1] * scale)
                l_s[head, at] = l_s[head, at] * alpha + jnp.sum(p, axis=1, keepdims=True)
                m_s[head, at] = m_new
                vals = jnp.concatenate([vb[part, a, b] for b in range(blocks)], axis=0)
                acc_s[head, at] = acc_s[head, at] * alpha + dot(p.astype(BF16), vals)
            return carry

        lax.fori_loop(0, tokens // q_tile, tile, 0)

    def kv_both(phase, step, then_phase, then_step):
        for part in (0, 1):
            kv_wait(part, phase, step)
            if then_phase is not None:
                kv_send(part, then_phase, then_step)

    kv_both(0, 1, 0, 2)
    kv_both(0, 2, 1, 1)
    for step in range(1, hz + 1):
        for e in (0, 1):
            if step == hz and e == 0:
                for i in (0, 1, 2):
                    own[i].wait()
            z_wait(e, step)
        if step == max(1, hz - 1):
            kv_both(1, 1, 1, 2)

    row_tile = 256 if rows % 256 == 0 else rows // 2
    f_width = wg.shape[2]

    def expert(e):
        dd_wait(e)

        def tile(t, carry):
            at = pl.ds(pl.multiple_of(t * row_tile, row_tile), row_tile)
            xx = jnp.concatenate([xbuf[e, i // 2, i % 2, at] for i in range(2 * nz)], axis=1)
            gate = dot(xx, wg[e])
            up = dot(xx, wu[e])
            hidden = (gate / (1.0 + jnp.exp(-gate)) * up).astype(BF16)
            part = dot(hidden, wd[e]).astype(BF16)
            for i in range(2 * nz):
                pbuf[e, i // 2, i % 2, at] = part[:, i * LANES : (i + 1) * LANES]
            return carry

        lax.fori_loop(0, rows // row_tile, tile, 0)
        send(pbuf.at[e, :, oc], sbuf.at[e], pss.at[e], psr.at[e], (ep, sib))

    def reducer(p, s, r, t, ssem, rsem):
        whole = p.shape[2]
        cut = whole // 2

        def term(dest, at):
            return p[dest, c, at].astype(F32) + s[dest, at].astype(F32)

        def put(step):
            for d, sign in ((0, 1), (1, -1)):
                dest = lax.rem(z + sign * (hz + 1 - step) + nz, nz)
                if step == 1:
                    at = pl.ds(d * cut, cut)
                    t[d, 0, at] = term(dest, at).astype(BF16)
                    piece, there = t.at[d, 0, at], r.at[d, 0, at]
                else:
                    for g in (0, 1):
                        at = pl.ds(g * cut, cut)
                        v = term(dest, at)
                        if step > 2 or g == d:
                            v = v + r[d, step - 2, at].astype(F32)
                        t[d, step - 1, at] = v.astype(BF16)
                    piece, there = t.at[d, step - 1], r.at[d, step - 1]
                send(piece, there, ssem.at[d, step - 1], rsem.at[d, step - 1], z_to[d])

        def take(step):
            for d in (0, 1):
                there = r.at[d, step - 1, pl.ds(d * cut, cut)] if step == 1 else r.at[d, step - 1]
                arrived(there, ssem.at[d, step - 1], rsem.at[d, step - 1], z_to[1 - d])

        def last():
            out = []
            for g in (0, 1):
                at = pl.ds(g * cut, cut)
                v = term(z, at)
                for d in (0, 1):
                    if hz > 1 or g == d:
                        v = v + r[d, hz - 1, at].astype(F32)
                out.append(v.astype(BF16))
            return out

        return put, take, last

    def finish(e, last):
        for g, v in enumerate(last()):
            fin[e, g * hr : (g + 1) * hr] = v
        for k in range(1, ep_n):
            to = lax.rem(ep + k, ep_n)
            src = fin.at[e, pl.ds(pl.multiple_of(to * cap, 16), cap)]
            send(src, ret.at[2 * ep + e], bks.at[e, k], bkr.at[e, k], (to, tp))
        ret[2 * ep + e] = fin[e, mine]

    a0 = (y, x)
    alen = (ny, nx)
    order = [(part, i) for i in range(max(ny, nx)) for part in (0, 1) if i < alen[part]]
    todo = list(order)

    def some(count=1):
        for _ in range(count):
            if todo:
                part, i = todo.pop(0)
                off = (i + 1) // 2 if i % 2 else alen[part] - i // 2
                unit(part, lax.rem(a0[part] + off, alen[part]))

    expert(0)
    expert(1)
    kv_both(1, 2, None, None)
    red = [
        reducer(pbuf.at[e], sbuf.at[e], rbuf.at[e], tbuf.at[e], rss.at[e], rsr.at[e]) for e in (0, 1)
    ]
    for e in (0, 1):
        arrived(sbuf.at[e], pss.at[e], psr.at[e], (ep, sib))
        red[e][0](1)
    for step in range(1, hz + 1):
        for e in (0, 1):
            some()
            red[e][1](step)
            if step < hz:
                red[e][0](step + 1)
            else:
                finish(e, red[e][2])
    some(len(todo))

    lane = lax.broadcasted_iota(jnp.int32, (tokens, LANES), 1)
    attended = jnp.where(lane < VDIM, acc_s[0] / l_s[0], acc_s[1] / l_s[1]).astype(BF16)
    proj = dot(attended, wo_ref[...]).astype(BF16)
    per = tokens // (2 * nz)
    for i in range(2 * nz):
        ap[i // 2, i % 2] = proj[i * per : (i + 1) * per]
    send(ap.at[:, oc], asb, aps, apr, (ep, sib))
    put, take, last = reducer(ap, asb, arb, atb, ars, arr)
    arrived(asb, aps, apr, (ep, sib))
    put(1)
    for step in range(1, hz + 1):
        take(step)
        if step < hz:
            put(step + 1)
    for g, v in enumerate(last()):
        mixer_ref[g * (per // 2) : (g + 1) * (per // 2)] = v

    for e in (0, 1):
        for k in range(1, ep_n):
            frm = lax.rem(ep + ep_n - k, ep_n)
            arrived(ret.at[2 * frm + e], bks.at[e, k], bkr.at[e, k], (frm, tp))
    slot_count = 2 * ep_n * cap
    where_at = lax.broadcasted_iota(jnp.int32, (tokens, slot_count), 1)
    rets = ret[...].reshape(slot_count, LANES)
    total = jnp.zeros((tokens, LANES), F32)
    for k in (0, 1):
        pick = (where_at == slot_ref[:, k : k + 1]).astype(F32).astype(BF16)
        total = total + dot(pick, rets) * rw_ref[:, k : k + 1]
    expert_ref[...] = total.astype(BF16)

    for d in pending:
        d.wait_send()


def rotary_tables(tokens):
    half_width = ROPE // 2
    positions = (lax.axis_index("ep") * tokens + jnp.arange(tokens, dtype=jnp.int32)).astype(F32)
    frequencies = ROTARY_BASE ** (-jnp.arange(half_width, dtype=F32) / half_width)
    angles = positions[:, None] * frequencies[None, :]
    return jnp.cos(angles), jnp.sin(angles)


def local(
    dims,
    query_latent, joint_latent, rotary_key, query_gain, joint_gain, query_weight, query_rotary,
    key_weight, value_weight, output_weight, expert_input, expert_gain, routes, route_weight,
    gate_weight, up_weight, down_weight,
):
    ny, nx, nz = dims
    ep_n, tokens, width = ny * nx, query_latent.shape[0], output_weight.shape[1]
    cap = 3 * tokens // (2 * ep_n)
    experts = 2 * ep_n
    rows = ep_n * cap
    half = tokens // 2
    hw = ROPE // 2

    cos, sin = rotary_tables(tokens)
    k1, k2 = rotary_key[:, :hw].astype(F32), rotary_key[:, hw:].astype(F32)
    turned_t = jnp.concatenate([k1 * cos - k2 * sin, k2 * cos + k1 * sin], axis=1).astype(BF16).T

    def placed(plain0, rope0, rope1, plain1, n):
        pad = jnp.zeros((n, ROPE), plain0.dtype)
        return jnp.concatenate([plain0, rope0, pad, pad, rope1, plain1], axis=1)

    def swapped(w):
        return jnp.concatenate([w[:, hw:], w[:, :hw]], axis=1)

    depth = query_weight.shape[0]
    none = jnp.zeros((depth, NOPE), BF16)
    wa = placed(query_weight[:, :NOPE], query_rotary[:, :ROPE], query_rotary[:, ROPE:], query_weight[:, NOPE:], depth)
    wb = placed(none, swapped(query_rotary[:, :ROPE]), swapped(query_rotary[:, ROPE:]), none, depth)
    cc = jnp.concatenate([cos, cos], axis=1)
    ss = jnp.concatenate([-sin, sin], axis=1)
    one = jnp.ones((tokens, NOPE), F32)
    cq = placed(one, cc, cc, one, tokens)
    sq = placed(one * 0, ss, ss, one * 0, tokens)

    sds = jax.ShapeDtypeStruct
    slots, kt_own, v_own, q, slot = pl.pallas_call(
        functools.partial(front_kernel, cap, experts),
        out_shape=(
            sds((experts, cap, LANES), BF16),
            sds((2, LANES + ROPE, half), BF16),
            sds((2, half, LANES), BF16),
            sds((tokens, 2 * LANES), BF16),
            sds((tokens, 2), jnp.int32),
        ),
        compiler_params=pltpu.CompilerParams(vmem_limit_bytes=56 * 2**20),
        name="front",
    )(
        query_latent, joint_latent, turned_t, query_gain[None], joint_gain[None], wa, wb, cq, sq,
        key_weight.T, value_weight, expert_input, expert_gain[None], routes, routes.T,
    )
    slots = slots.reshape(ep_n, 2, cap, LANES)

    hz = nz // 2
    per = tokens // (2 * nz)
    vmem = pl.BlockSpec(memory_space=pltpu.VMEM)
    hbm = pl.BlockSpec(memory_space=pl.ANY)
    sem = pltpu.SemaphoreType.DMA
    scratch = [
        pltpu.VMEM((2, nz, 2, rows, LANES), BF16),
        pltpu.VMEM((2, nz, 2, rows, LANES), BF16),
        pltpu.VMEM((2, nz, rows, LANES), BF16),
        pltpu.VMEM((2, 2, hz, rows, LANES), BF16),
        pltpu.VMEM((2, 2, hz, rows, LANES), BF16),
        pltpu.VMEM((2, rows, LANES), BF16),
        pltpu.VMEM((experts, cap, LANES), BF16),
        pltpu.VMEM((2, max(ny, nx), max(ny, nx), LANES + ROPE, half), BF16),
        pltpu.VMEM((2, max(ny, nx), max(ny, nx), half, LANES), BF16),
        pltpu.VMEM(gate_weight.shape, BF16),
        pltpu.VMEM(up_weight.shape, BF16),
        pltpu.VMEM(down_weight.shape, BF16),
        pltpu.VMEM((2, tokens, LANES), F32),
        pltpu.VMEM((2, tokens, LANES), F32),
        pltpu.VMEM((2, tokens, LANES), F32),
        pltpu.VMEM((nz, 2, per, width), BF16),
        pltpu.VMEM((nz, per, width), BF16),
        pltpu.VMEM((2, hz, per, width), BF16),
        pltpu.VMEM((2, hz, per, width), BF16),
        sem((ep_n,)), sem((ep_n,)),
        sem((2, 2, hz)), sem((2, 2, hz)),
        sem((2, 2, hz + 1)), sem((2, 2, hz + 1)),
        sem((2, 2, 2, 2, 2)), sem((2, 2, 2, 2, 2)),
        sem((2,)), sem((2,)),
        sem((2, 2, hz)), sem((2, 2, hz)),
        sem((2, ep_n)), sem((2, ep_n)),
        sem(()), sem(()),
        sem((2, hz)), sem((2, hz)),
        sem((8,)),
    ]
    mixer, expert = pl.pallas_call(
        functools.partial(main_kernel, (ny, nx, nz, cap)),
        out_shape=(sds((per, width), BF16), sds((tokens, LANES), BF16)),
        in_specs=[vmem, hbm, hbm, vmem, vmem, vmem, hbm, hbm, hbm, vmem],
        out_specs=(vmem, vmem),
        scratch_shapes=scratch,
        compiler_params=pltpu.CompilerParams(
            collective_id=0, has_side_effects=True, vmem_limit_bytes=62 * 2**20
        ),
        name="main",
    )(slots, kt_own, v_own, q, slot, route_weight, gate_weight, up_weight, down_weight, output_weight)
    return mixer, expert


def solution(mesh):
    ny, nx = ep_grid(mesh.shape["ep"])
    return jax.shard_map(
        functools.partial(local, (ny, nx, mesh.shape["tp"] // 2)),
        mesh=mesh,
        in_specs=(
            P("ep", None),
            P("ep", None),
            P("ep", None),
            P(),
            P(),
            P(None, "tp"),
            P(None, "tp"),
            P(None, "tp"),
            P(None, "tp"),
            P("tp", None),
            P("ep", None),
            P(),
            P("ep", None),
            P("ep", None),
            P("ep", None, "tp"),
            P("ep", None, "tp"),
            P("ep", "tp", None),
        ),
        out_specs=(P(("ep", "tp"), None), P("ep", "tp")),
        check_vma=False,
    )
```

time: 356 us -> 141 us (0.40)
  Pallas kernels: 0 us -> 120 us
  waiting for transfers between devices: 110 us -> 0 us
  matrix products: 88 us -> 0 us
  local copies, waits for them, and re-layouts: 88.7 us -> 15.8 us
  other arithmetic: 27.5 us -> 2.83 us
  blocking collectives: 16.6 us -> 0 us
  between operations: 14.3 us -> 0.81 us
  starting transfers between devices: 5.52 us -> 0 us
    pallas_call x0 -> x2, Pallas kernels: none -> 120 us  [the longest x1 114 us: local(): pl.pallas_call(functools.partial(main_kernel, (ny, nx, nz, cap)), out_sha...]
    dot_general x85 -> x0, matrix products: 88 us -> none  [the longest x16 21.7 us: scan_step(): jnp.dot(latent_block, value_weight, preferred_element_type=jnp.float32)]
    all_gather x2 -> x0, waiting for transfers between devices: 67.7 us -> none  [the longest x1 50.7 us: experts(): piece = lax.all_gather(arrived, 'tp', axis=3, tiled=True)]
    unnamed x38 -> x19, local copies, waits for them, and re-layouts: 56.3 us -> 5.98 us
    reduce_scatter x1 -> x0, waiting for transfers between devices: 32.9 us -> none  [token_mixer(): lax.psum_scatter(jnp.dot(attended, output_weight, preferred_element_type=...]
    all_to_all x1 -> x0, blocking collectives: 16.6 us -> none  [experts(): lax.all_to_all(outgoing, 'ep', split_axis=0, concat_axis=0, tiled=True)]
    scatter x2 -> x0, local copies, waits for them, and re-layouts: 11.9 us -> none  [the longest x1 7.59 us: experts(): jnp.zeros((expert_count * capacity,), jnp.bfloat16).at[slot_index].set(1.0)]
    reduce_sum x21 -> x0, other arithmetic: 9.29 us -> none  [the longest x16 4.85 us: attend_block(): row_total = row_total * factor + jnp.sum(expo, axis=-1)]
  transfers between devices with their start and end apart: 5 -> 0, of which waited for: 4 -> 0; matrix products, arithmetic and copies ran while one was open for 48% -> 0% of each run, Pallas kernels for 0% -> 0%
where the time goes in v1:
time: 141 us; the launch traced here: 139 us
  Pallas kernels  120 us (85%)
  local copies, waits for them, and re-layouts  15.8 us (11%)
  other arithmetic  2.83 us (2%)
    pallas_call x1, Pallas kernels, local(): pl.pallas_call(functools.partial(main_kernel, (ny, nx, nz, cap)), out_sha...  114 us
    concatenate x4, local copies, waits for them, and re-layouts, placed(): return jnp.concatenate([plain0, rope0, pad, pad, rope1, plain1], axis=1)  7.72 us
    pallas_call x1, Pallas kernels, local(): pl.pallas_call(functools.partial(front_kernel, cap, experts), out_shape=(...  6.02 us
    unnamed x19, local copies, waits for them, and re-layouts  5.98 us

profile of v1, /device:TPU:1, one launch (start us, length us, event | category | flops | bytes accessed | tf_op | source)
XLA Modules:
  0.0 139.2 jit_solution(14873935584233840163)
XLA Ops:
  0.6 0.8 fusion.5
  1.5 0.2 copy.51
  1.6 0.2 copy.52
  1.8 0.2 copy.53
  2.0 0.2 copy.54
  2.2 3.6 %concatenate.22.wb = bf16[1024,256]{1,0:T(8,128)(2,1)} concatenate(bf16[1024,64]{1,0:T(8,128)(2,1)S(1)} %broadcast.27, bf16[1024,16]{1,0:T(8,128)(2,1)S(1)} %copy.51, bf16[1024,16]{1,0:T(8,128)(2,1)S(1)} %copy.52, bf16[1024,64]{1,0:T(8,128)(2,1)S(1)} %broadcast.27, bf16[1024,16]{1,0:T(8,128)(2,1)S(1)} %copy.53, bf16[1024,16]{1,0:T(8,128)(2,1)S(1)} %copy.54, ...), dimensions={1} | concatenate | bytes 1048576 | tf_op jit(solution)/shard_map/concatenate | solution.py:449
  5.8 0.1 copy.44
  6.0 0.1 copy.45
  6.1 1.2 fusion.3
  7.5 0.6 maximum_bitcast_fusion.rk_t
  8.1 1.0 multiply_sine_fusion
  9.1 1.4 %concatenate.24.sq = f32[512,256]{1,0:T(8,128)} concatenate(f32[512,64]{1,0:T(8,128)S(1)} %broadcast.28, f32[512,16]{1,0:T(8,128)S(1)} %get-tuple-element.25, f32[512,16]{1,0:T(8,128)S(1)} %get-tuple-element.24, f32[512,64]{1,0:T(8,128)S(1)} %broadcast.28, f32[512,16]{1,0:T(8,128)S(1)} %get-tuple-element.25, f32[512,16]{1,0:T(8,128)S(1)} %get-tuple-element.24, ...), dimensions={1} | concatenate | bytes 1048576 | tf_op jit(solution)/shard_map/concatenate | solution.py:449
  10.6 0.1 fusion.4
  10.7 0.2 copy.58
  10.9 0.2 copy.59
  11.1 1.3 concatenate.21.wa
  12.4 1.4 %concatenate.23.cq = f32[512,256]{1,0:T(8,128)} concatenate(f32[512,64]{1,0:T(8,128)S(1)} %broadcast_in_dim.16, f32[512,16]{1,0:T(8,128)S(1)} %get-tuple-element.26, f32[512,16]{1,0:T(8,128)S(1)} %get-tuple-element.26, f32[512,64]{1,0:T(8,128)S(1)} %broadcast.28, f32[512,16]{1,0:T(8,128)S(1)} %get-tuple-element.26, f32[512,16]{1,0:T(8,128)S(1)} %get-tuple-element.26, ...), dimensions={1} | concatenate | bytes 1048576 | tf_op jit(solution)/shard_map/concatenate | solution.py:449
  13.8 0.9 copy.56.routes
  14.7 0.8 copy.55
  15.5 6.0 %front.1 = (bf16[32,48,128]{2,1,0:T(8,128)(2,1)}, bf16[2,160,256]{2,1,0:T(8,128)(2,1)}, bf16[2,256,128]{2,1,0:T(8,128)(2,1)}, bf16[512,256]{1,0:T(8,128)(2,1)}, s32[512,2]{1,0:T(8,128)}) custom-call(bf16[512,1024]{1,0:T(8,128)(2,1)} %ql.1, bf16[512,512]{1,0:T(8,128)(2,1)} %jl.1, bf16[32,512]{1,0:T(8,128)(2,1)} %maximum_bitcast_fusion.rk_t, ...), custom_call_target="tpu_custom_call" | custom-call | tf_op jit(solution)/shard_map/front/pallas_call | solution.py:465
  21.5 0.9 copy.57.rw_ref
  22.3 113.7 %main.1 = (bf16[32,2048]{1,0:T(8,128)(2,1)}, bf16[512,128]{1,0:T(8,128)(2,1)}) custom-call(bf16[16,2,48,128]{3,2,1,0:T(8,128)(2,1)} %bitcast.9, bf16[2,160,256]{2,1,0:T(8,128)(2,1)} %get-tuple-element.8.kt_own, bf16[2,256,128]{2,1,0:T(8,128)(2,1)} %get-tuple-element.9.v_own, bf16[512,256]{1,0:T(8,128)(2,1)} %get-tuple-element.10.q_ref, ...), custom_call_target="tpu_custom_call" | custom-call | tf_op jit(solution)/shard_map/main/pallas_call | solution.py:518
  136.0 1.6 %copy.62 = bf16[32,2048]{1,0:T(8,128)(2,1)} copy(bf16[32,2048]{1,0:T(8,128)(2,1)} %get-tuple-element.29) | data formatting | bytes 262144
  137.6 1.6 %copy.63 = bf16[512,128]{1,0:T(8,128)(2,1)} copy(bf16[512,128]{1,0:T(8,128)(2,1)} %get-tuple-element.30) | data formatting | bytes 262144
  (21 shorter events, 0.3 us)
Async XLA Ops:
  0.6 5.2 %copy-start.3 = (bf16[512,32]{0,1:T(8,128)(2,1)S(1)}, bf16[512,32]{0,1:T(8,128)(2,1)}, u32[]{:S(2)}) copy-start(bf16[512,32]{0,1:T(8,128)(2,1)} %param.19) | copy-start | bytes 98308
  6.1 4.5 %copy-start = (bf16[1024,128]{1,0:T(8,128)(2,1)S(1)}, bf16[1024,128]{1,0:T(8,128)(2,1)}, u32[]{:S(2)}) copy-start(bf16[1024,128]{1,0:T(8,128)(2,1)} %param.22) | copy-start | bytes 786436
  8.1 2.6 %copy-start.1 = (bf16[1024,64]{0,1:T(8,128)(2,1)S(1)}, bf16[1024,64]{0,1:T(8,128)(2,1)}, u32[]{:S(2)}) copy-start(bf16[1024,64]{0,1:T(8,128)(2,1)} %param.23) | copy-start | bytes 393220
  11.1 2.8 %copy-start.4 = (s32[512,2]{0,1:T(2,128)S(1)}, s32[512,2]{0,1:T(2,128)}, u32[]{:S(2)}) copy-start(s32[512,2]{0,1:T(2,128)} %param.29) | copy-start | bytes 12292
  11.1 3.6 %copy-start.2 = (bf16[512,128]{1,0:T(8,128)(2,1)S(1)}, bf16[512,128]{1,0:T(8,128)(2,1)}, u32[]{:S(2)}) copy-start(bf16[512,128]{1,0:T(8,128)(2,1)} %param.24) | copy-start | bytes 393220
  15.5 6.0 %copy-start.5 = (f32[512,2]{0,1:T(2,128)S(1)}, f32[512,2]{0,1:T(2,128)}, u32[]{:S(2)}) copy-start(f32[512,2]{0,1:T(2,128)} %param.30) | copy-start | bytes 12292

commit v2 on v1

v2 whole, which is shorter than its diff:
```python
import functools

import jax
import jax.numpy as jnp
from jax import lax
from jax.experimental import pallas as pl
from jax.experimental.pallas import tpu as pltpu
from jax.sharding import PartitionSpec as P

NOPE = 64
VDIM = 64
ROPE = 32
NORM_EPSILON = 1e-06
ROTARY_BASE = 10000.0
LANES = 128
LOG2E = 1.4426950408889634
MESH = pl.DeviceIdType.MESH
F32 = jnp.float32
BF16 = jnp.bfloat16


def ep_grid(count):
    return {16: (4, 4), 4: (2, 2), 2: (1, 2)}[count]


def dot(a, b):
    return jnp.dot(a, b, preferred_element_type=F32)


def dot_nt(a, b):
    return lax.dot_general(a, b, (((1,), (1,)), ((), ())), preferred_element_type=F32)


def main_kernel(
    dims,
    routes_ref, rw_ref, qgain, jgain, egain, rk_ref, cos_ref, sin_ref,
    xin_hbm, jl_hbm, wk_hbm, wv_hbm, ql_hbm, wq_hbm, wr_hbm, wg_hbm, wu_hbm, wd_hbm, wo_hbm,
    mixer_ref, expert_ref,
    xin, jl, wk, wv, ql, wq, wr, wg, wu, wd, wo,
    slots, xbuf, pbuf, sbuf, rbuf, tbuf, fin, ret, ktb, vb, q_s, cols, m_s, l_s, acc_s,
    ap, asb, arb, atb,
    a2a_s, a2a_r, zs, zr, dds, ddr, kvs, kvr, pss, psr, rss, rsr, bks, bkr, aps, apr, ars, arr, local_s, own_s,
):
    ny, nx, nz, cap = dims
    ep_n = ny * nx
    experts = 2 * ep_n
    rows = ep_n * cap
    ns = nz // 2
    ep = lax.axis_index("ep")
    tp = lax.axis_index("tp")
    y, x = ep // nx, lax.rem(ep, nx)
    z, c = tp // 2, lax.rem(tp, 2)
    par = lax.rem(z, 2)
    opar = 1 - par
    oc = 1 - c
    zright = lax.rem(z + 1, nz)
    zleft = lax.rem(z + nz - 1, nz)
    z_to = ((ep, zright * 2 + c), (ep, zleft * 2 + c))
    sib = (ep, z * 2 + oc)
    tokens = xin.shape[0]
    half = tokens // 2
    pending = []

    def send(src, dst, ssem, rsem, to):
        d = pltpu.make_async_remote_copy(
            src_ref=src, dst_ref=dst, send_sem=ssem, recv_sem=rsem, device_id=to, device_id_type=MESH
        )
        d.start()
        pending.append(d)

    def arrived(dst, ssem, rsem, frm):
        pltpu.make_async_remote_copy(
            src_ref=dst, dst_ref=dst, send_sem=ssem, recv_sem=rsem, device_id=frm, device_id_type=MESH
        ).wait_recv()

    barrier = pltpu.get_barrier_semaphore()
    peers = [(lax.rem(ep + k, ep_n), tp) for k in range(1, ep_n)]
    peers.append(sib)
    peers.append(z_to[0])
    if nz > 2:
        peers.append(z_to[1])
    for peer in peers:
        pl.semaphore_signal(barrier, inc=1, device_id=peer, device_id_type=MESH)

    loads = {}
    for i, (name, src, dst) in enumerate(
        (
            ("xin", xin_hbm, xin), ("jl", jl_hbm, jl), ("wk", wk_hbm, wk), ("wv", wv_hbm, wv),
            ("ql", ql_hbm, ql), ("wq", wq_hbm, wq), ("wr", wr_hbm, wr), ("wg", wg_hbm, wg),
            ("wu", wu_hbm, wu), ("wd", wd_hbm, wd), ("wo", wo_hbm, wo),
        )
    ):
        loads[name] = pltpu.make_async_copy(src, dst, local_s.at[i])
        loads[name].start()

    with jax.named_scope("routing"):
        row = lax.broadcasted_iota(jnp.int32, (tokens, tokens), 0)
        col = lax.broadcasted_iota(jnp.int32, (tokens, tokens), 1)
        sub_e = lax.broadcasted_iota(jnp.int32, (experts, tokens), 0)
        named0 = sub_e == routes_ref[0:1, :]
        named1 = sub_e == routes_ref[1:2, :]
        named = named0 | named1
        before = dot(named.astype(F32).astype(BF16), (row < col).astype(F32).astype(BF16))
        rank = jnp.where(named, before, -1.0)
        place = before + (sub_e * cap).astype(F32)
        slot0 = jnp.sum(jnp.where(named0, place, 0.0), axis=0, keepdims=True)
        slot1 = jnp.sum(jnp.where(named1, place, 0.0), axis=0, keepdims=True)
        stack = jnp.concatenate([slot0, slot1, rw_ref[...], jnp.zeros((4, tokens), F32)], axis=0)
        cols[...] = stack.T

    with jax.named_scope("expert_norm"):
        loads["xin"].wait()
        xf = xin[...].astype(F32)
        factor = lax.rsqrt(jnp.mean(xf * xf, axis=-1, keepdims=True) + NORM_EPSILON)
        mine = []
        for i in range(ns):
            at = pl.ds(pl.multiple_of((4 * i + 2 * par + c) * LANES, LANES), LANES)
            mine.append((xin[:, at].astype(F32) * factor * egain[:, at]).astype(BF16))
        mine = jnp.concatenate(mine, axis=1)
        place_in = lax.broadcasted_iota(jnp.int32, (cap, tokens), 0).astype(F32)

    groups = [pl.ds(0, ns)] if ns == 1 else [pl.ds(0, ns // 2), pl.ds(ns // 2, ns - ns // 2)]
    members = [range(g.start, g.start + g.size) for g in groups]
    mine_rows = pl.ds(pl.multiple_of(ep * cap, 16), cap)

    def dispatch(e):
        group = min(8, ep_n)
        with jax.named_scope("slots"):
            for d0 in range(0, ep_n, group):
                pick = [
                    (place_in == rank[2 * d + e : 2 * d + e + 1, :]).astype(F32).astype(BF16)
                    for d in range(d0, d0 + group)
                ]
                out = dot(jnp.concatenate(pick, axis=0), mine).astype(BF16)
                for d in range(group):
                    for i in range(ns):
                        slots[e, d0 + d, i] = out[d * cap : (d + 1) * cap, i * LANES : (i + 1) * LANES]
        if e == 0:
            with jax.named_scope("barrier"):
                pl.semaphore_wait(barrier, len(peers))
        for g, span in enumerate(groups):
            for k in range(1, ep_n):
                to = lax.rem(ep + k, ep_n)
                there = xbuf.at[e, span, par, c, mine_rows]
                send(slots.at[e, to, span], there, a2a_s.at[e, g, k], a2a_r.at[e, g, k], (to, tp))
        pltpu.make_async_copy(slots.at[e, ep], xbuf.at[e, :, par, c, mine_rows], own_s.at[e]).start()

    axes = (("x", nx, x), ("y", ny, y))

    def ring_to(name, step):
        if name == "x":
            return (y * nx + lax.rem(x + nx + step, nx), tp)
        return (lax.rem(y + ny + step, ny) * nx + x, tp)

    def kv_refs(part, phase, block, j):
        other = (y, x)[part]
        if phase == 0:
            return ktb.at[part, other, block], vb.at[part, other, block]
        n, me = ((nx, x), (ny, y))[part]
        b = lax.rem(me + j, n)
        return ktb.at[part, block, b], vb.at[part, block, b]

    def kv_copies(part, phase, step, j, arriving):
        name, n, me = axes[(part + phase) % 2]
        if n == 1 or step > n // 2:
            return
        tie = 2 * step == n
        for d, sign in ((0, 1), (1, -1)):
            block = lax.rem(me + n - sign * (step if arriving else step - 1), n)
            refs = kv_refs(part, phase, block, j)
            for kind in (0, 1):
                if not tie or kind == d:
                    i = (part, phase * 4 + j, d, step - 1, kind)
                    if arriving:
                        arrived(refs[kind], kvs.at[i], kvr.at[i], ring_to(name, -sign))
                    else:
                        send(refs[kind], refs[kind], kvs.at[i], kvr.at[i], ring_to(name, sign))

    def kv_js(part, step):
        n = (nx, ny)[part]
        return ([0], sorted({1, n - 1} - {0, n}), [2] if n == 4 else [])[step]

    def kv_line(step):
        with jax.named_scope(f"kv_line#s={step}"):
            for part in (0, 1):
                if step:
                    kv_copies(part, 0, step, 0, True)
                kv_copies(part, 0, step + 1, 0, False)
                for j in kv_js(part, step):
                    kv_copies(part, 1, 1, j, False)

    def kv_plane(step, pieces):
        with jax.named_scope(f"kv_plane#s={step}"):
            for part in (0, 1):
                for piece in pieces:
                    for j in kv_js(part, piece):
                        kv_copies(part, 1, step, j, True)
                        kv_copies(part, 1, step + 1, j, False)

    def normed(ref, gain):
        v = ref[...].astype(F32)
        f = lax.rsqrt(jnp.mean(v * v, axis=-1, keepdims=True) + NORM_EPSILON)
        return (v * f * gain[...]).astype(BF16)

    lane = lax.broadcasted_iota(jnp.int32, (tokens, LANES), 1)
    scale = LOG2E * (NOPE + ROPE) ** (-0.5)

    def turned(u):
        left = pltpu.roll(u, LANES - ROPE // 2, 1)
        right = pltpu.roll(u, ROPE // 2, 1)
        other = jnp.where(lax.rem(lane, ROPE) < ROPE // 2, left, right)
        return u * cos_ref[...] + other * sin_ref[...]

    def keys_values():
        with jax.named_scope("kv_proj"):
            for name in ("jl", "wk", "wv"):
                loads[name].wait()
            jn = normed(jl, jgain)
            kt = dot(jn, wk[...]).T.astype(BF16)
            wide = jnp.concatenate([rk_ref[...].astype(F32), jnp.zeros((LANES - ROPE, tokens), F32)], axis=0)
            rt = turned(wide.T).T[0:ROPE].astype(BF16)
            vv = dot(jn, wv[...]).astype(BF16)
            for h, (a, b) in enumerate(((y, x), (x, y))):
                part = slice(h * half, (h + 1) * half)
                ktb[h, a, b, 0:NOPE, :] = kt[0:NOPE, part]
                ktb[h, a, b, NOPE : NOPE + ROPE, :] = rt[:, part]
                ktb[h, a, b, NOPE + ROPE :, :] = kt[NOPE:, part]
                vb[h, a, b] = vv[part]
        kv_line(0)

    def queries():
        with jax.named_scope("q_proj"):
            for name in ("ql", "wq", "wr"):
                loads[name].wait()
            qn = normed(ql, qgain)
            plain = dot(qn, wq[...])
            rope = dot_nt(qn, wr[...])
            rope = turned(jnp.concatenate([rope, jnp.zeros((tokens, LANES - 2 * ROPE), F32)], axis=1))
            first = jnp.where(lane < NOPE, plain, jnp.where(lane < NOPE + ROPE, pltpu.roll(rope, NOPE, 1), 0.0))
            second = jnp.where(lane < ROPE, 0.0, jnp.where(lane < NOPE, rope, plain))
            q_s[0] = (first * scale).astype(BF16)
            q_s[1] = (second * scale).astype(BF16)

    def a2a_wait(e, g):
        if g >= len(groups):
            return
        span = groups[g]
        with jax.named_scope(f"a2a_wait#e={e}#g={g}"):
            if g == 0:
                pltpu.make_async_copy(slots.at[e, ep], xbuf.at[e, :, par, c, mine_rows], own_s.at[e]).wait()
            for k in range(1, ep_n):
                frm = lax.rem(ep + ep_n - k, ep_n)
                there = xbuf.at[e, span, par, c, pl.ds(pl.multiple_of(frm * cap, 16), cap)]
                arrived(there, a2a_s.at[e, g, k], a2a_r.at[e, g, k], (frm, tp))
        for i in members[g]:
            piece = xbuf.at[e, i, par, c]
            send(piece, piece, zs.at[e, i], zr.at[e, i], z_to[i % 2])
        piece = xbuf.at[e, span, par, c]
        send(piece, piece, dds.at[e, ns + g], ddr.at[e, ns + g], sib)

    def z_wait(e, g):
        if g >= len(groups):
            return
        with jax.named_scope(f"z_wait#e={e}#g={g}"):
            for i in members[g]:
                piece = xbuf.at[e, i, opar, c]
                arrived(piece, zs.at[e, i], zr.at[e, i], z_to[1 - i % 2])
                send(piece, piece, dds.at[e, i], ddr.at[e, i], sib)

    row_tile = 256 if rows % 256 == 0 else rows // 2

    def pair_copy(e, t):
        at = pl.ds(pl.multiple_of(t * row_tile, row_tile), row_tile)
        return pltpu.make_async_remote_copy(
            src_ref=pbuf.at[e, :, oc, at], dst_ref=sbuf.at[e, :, at], send_sem=pss.at[e, t], recv_sem=psr.at[e, t],
            device_id=sib, device_id_type=MESH,
        )

    def expert(e):
        with jax.named_scope(f"dd_wait#e={e}"):
            for g, span in enumerate(groups):
                arrived(xbuf.at[e, span, par, oc], dds.at[e, ns + g], ddr.at[e, ns + g], sib)
            for i in range(ns):
                arrived(xbuf.at[e, i, opar, oc], dds.at[e, i], ddr.at[e, i], sib)

        def tile(t, carry):
            at = pl.ds(pl.multiple_of(t * row_tile, row_tile), row_tile)
            xx = jnp.concatenate([xbuf[e, j // 4, j // 2 % 2, j % 2, at] for j in range(2 * nz)], axis=1)
            gate = dot(xx, wg[e])
            up = dot(xx, wu[e])
            hidden = (gate / (1.0 + jnp.exp(-gate)) * up).astype(BF16)
            part = dot(hidden, wd[e]).astype(BF16)
            for j in range(2 * nz):
                pbuf[e, j // 2, j % 2, at] = part[:, j * LANES : (j + 1) * LANES]
            pair_copy(e, t).start()
            return carry

        with jax.named_scope(f"expert#e={e}"):
            lax.fori_loop(0, rows // row_tile, tile, 0)
        for t in range(rows // row_tile):
            pending.append(pair_copy(e, t))

    hz = nz // 2

    def reducer(name, p, s, r, t, ssem, rsem):
        cut = p.shape[2] // 2

        def term(dest, at):
            return p[dest, c, at].astype(F32) + s[dest, at].astype(F32)

        def put(own, step):
            if step > hz:
                return
            for d, sign in ((0, 1), (1, -1)):
                g = d if own else 1 - d
                at = pl.ds(g * cut, cut)
                dest = lax.rem(z + sign * (hz + 1 - step) + nz, nz)
                v = term(dest, at)
                if step > (1 if own else 2):
                    v = v + r[d, step - 2, at].astype(F32)
                t[d, step - 1, at] = v.astype(BF16)
                i = (d, g, step - 1)
                send(t.at[d, step - 1, at], r.at[d, step - 1, at], ssem.at[i], rsem.at[i], z_to[d])

        def take(own, step):
            for d in (0, 1):
                g = d if own else 1 - d
                at = pl.ds(g * cut, cut)
                i = (d, g, step - 1)
                arrived(r.at[d, step - 1, at], ssem.at[i], rsem.at[i], z_to[1 - d])

        events = []
        for step in range(1, hz + 1):
            events.append((True, step))
            if step < hz:
                events.append((False, step + 1))

        def start():
            with jax.named_scope(f"start#{name}"):
                put(True, 1)
                put(False, 2)

        def event():
            own, step = events.pop(0)
            with jax.named_scope(f"take#{name}#own={int(own)}#s={step}"):
                take(own, step)
            put(own, step + 1)

        def last():
            out = []
            for g in (0, 1):
                at = pl.ds(g * cut, cut)
                v = term(z, at)
                for d in (0, 1):
                    if hz > 1 or g == d:
                        v = v + r[d, hz - 1, at].astype(F32)
                out.append(v.astype(BF16))
            return out

        return start, event, last, events

    hr = rows // 2

    def finish(e, last):
        with jax.named_scope(f"finish#e={e}"):
            for g, v in enumerate(last()):
                fin[e, g * hr : (g + 1) * hr] = v
            for k in range(1, ep_n):
                to = lax.rem(ep + k, ep_n)
                src = fin.at[e, pl.ds(pl.multiple_of(to * cap, 16), cap)]
                send(src, ret.at[2 * ep + e], bks.at[e, k], bkr.at[e, k], (to, tp))
            ret[2 * ep + e] = fin[e, mine_rows]

    q_tile = min(256, tokens)

    def unit(part, a):
        blocks = (nx, ny)[part]

        def tile(t):
            at = pl.ds(t * q_tile, q_tile)
            both = []
            for head in (0, 1):
                q = q_s[head, at]
                both.append([dot(q, ktb[part, a, b, head * ROPE : head * ROPE + LANES, :]) for b in range(blocks)])
            vals = jnp.concatenate([vb[part, a, b] for b in range(blocks)], axis=0)
            for head, s in enumerate(both):
                m_old = m_s[head, at]
                m_new = jnp.maximum(m_old, jnp.max(functools.reduce(jnp.maximum, s), axis=1, keepdims=True))
                alpha = jnp.exp2(m_old - m_new)
                m_s[head, at] = m_new
                p = [jnp.exp2(v[:, i : i + LANES] - m_new) for v in s for i in range(0, half, LANES)]
                l_s[head, at] = l_s[head, at] * alpha + functools.reduce(jnp.add, p)
                p = jnp.concatenate([v.astype(BF16) for v in p], axis=1)
                acc_s[head, at] = acc_s[head, at] * alpha + dot(p, vals)

        return tile

    a0 = (y, x)
    alen = (ny, nx)
    tiles = tokens // q_tile
    todo = []
    for near in ((0,), (1, 2), (3,)):
        pairs = [(part, i) for i in near for part in (0, 1) if i < alen[part]]
        if near == (3,) or max(alen) < 4:
            todo += [(part, i, t) for t in range(tiles) for part, i in pairs]
        else:
            todo += [(part, i, t) for part, i in pairs for t in range(tiles)]

    def some(count=1):
        for _ in range(count):
            if todo:
                part, i, t = todo.pop(0)
                off = (0, alen[part] - 1, 1, 2)[i] if alen[part] > 2 else i
                with jax.named_scope(f"unit#n={len(todo)}"):
                    unit(part, lax.rem(a0[part] + off, alen[part]))(t)

    red = [
        reducer(f"e{e}", pbuf.at[e], sbuf.at[e], rbuf.at[e], tbuf.at[e], rss.at[e], rsr.at[e]) for e in (0, 1)
    ]

    def pair(e):
        with jax.named_scope(f"pair#e={e}"):
            for t in range(rows // row_tile):
                pair_copy(e, t).wait_recv()

    def out_proj():
        with jax.named_scope("out_proj"):
            loads["wo"].wait()
            t0 = jnp.sum(l_s[0], axis=1, keepdims=True)
            t1 = jnp.sum(l_s[1], axis=1, keepdims=True)
            attended = jnp.where(lane < VDIM, acc_s[0] / t0, acc_s[1] / t1).astype(BF16)
            per = tokens // (2 * nz)
            for q in range(0, nz, hz):
                proj = dot(attended[q * 2 * per : (q + hz) * 2 * per], wo[...]).astype(BF16)
                for i in range(2 * hz):
                    ap[q + i // 2, i % 2] = proj[i * per : (i + 1) * per]
                span = pl.ds(q, hz)
                send(ap.at[span, oc], asb.at[span], aps.at[q // hz], apr.at[q // hz], sib)

    def combine():
        with jax.named_scope("combine_wait"):
            for e in (0, 1):
                for k in range(1, ep_n):
                    frm = lax.rem(ep + ep_n - k, ep_n)
                    arrived(ret.at[2 * frm + e], bks.at[e, k], bkr.at[e, k], (frm, tp))
        with jax.named_scope("combine"):
            slot_count = experts * cap
            where_at = lax.broadcasted_iota(jnp.int32, (tokens, slot_count), 1).astype(F32)
            rets = ret[...].reshape(slot_count, LANES)
            total = jnp.zeros((tokens, LANES), F32)
            for k in (0, 1):
                pick = (where_at == cols[:, k : k + 1]).astype(F32).astype(BF16)
                total = total + dot(pick, rets) * cols[:, 2 + k : 3 + k]
            expert_ref[...] = total.astype(BF16)

    red.append(reducer("a", ap, asb, arb, atb, ars, arr))

    def step_of(e):
        if red[e][3]:
            red[e][1]()
            if e < 2 and not red[e][3]:
                finish(e, red[e][2])

    kv_state = []

    def kv_upto(count):
        for stage in range(len(kv_state) + 1, count + 1):
            kv_state.append(stage)
            if stage == 1:
                kv_plane(1, (0, 1))
            elif stage == 2:
                kv_plane(1, (2,))
            else:
                kv_plane(2, (0, 1, 2))

    def work(count):
        for _ in range(count):
            if not todo:
                return
            if len(todo) <= 6 * tiles:
                kv_upto(2)
            if len(todo) <= 2 * tiles:
                kv_upto(3)
            some()

    dispatch(0)
    dispatch(1)
    keys_values()
    m_s[...] = jnp.full(m_s.shape, -jnp.inf, F32)
    l_s[...] = jnp.zeros(l_s.shape, F32)
    acc_s[...] = jnp.zeros(acc_s.shape, F32)
    queries()
    a2a_wait(0, 0)
    a2a_wait(0, 1)
    a2a_wait(1, 0)
    z_wait(0, 0)
    a2a_wait(1, 1)
    z_wait(0, 1)
    for name in ("wg", "wu", "wd"):
        loads[name].wait()
    expert(0)
    kv_line(1)
    z_wait(1, 0)
    pair(0)
    red[0][0]()
    z_wait(1, 1)
    expert(1)
    step_of(0)
    pair(1)
    red[1][0]()
    step_of(0)
    kv_line(2)
    work(1)
    step_of(0)
    work(1)
    step_of(0)
    work(2)
    step_of(1)
    kv_upto(1)
    step_of(1)
    step_of(0)
    kv_upto(2)
    work(2)
    for e in (0, 1, 1, 0):
        step_of(e)
        work(2)
    step_of(1)
    kv_upto(3)
    work(len(todo))
    out_proj()
    step_of(0)
    with jax.named_scope("pair#a"):
        for q in range(0, nz, hz):
            arrived(asb.at[pl.ds(q, hz)], aps.at[q // hz], apr.at[q // hz], sib)
    red[2][0]()
    for e in (1, 2, 1, 2, 1, 2, 2):
        step_of(e)
    for e in (0, 1):
        while red[e][3]:
            step_of(e)
    while len(red[2][3]) > 1:
        step_of(2)
    combine()
    while red[2][3]:
        step_of(2)
    cut = mixer_ref.shape[0] // 2
    for g, v in enumerate(red[2][2]()):
        mixer_ref[g * cut : (g + 1) * cut] = v

    for d in pending:
        d.wait_send()


def back_kernel(mixer, expert, mixer_out, expert_out):
    mixer_out[...] = mixer[...]
    expert_out[...] = expert[...]


def rotary_tables(tokens):
    half_width = ROPE // 2
    positions = (lax.axis_index("ep") * tokens + jnp.arange(tokens, dtype=jnp.int32)).astype(F32)
    lanes = jnp.arange(LANES, dtype=jnp.int32) % ROPE
    frequencies = ROTARY_BASE ** (-(lanes % half_width).astype(F32) / half_width)
    angles = positions[:, None] * frequencies[None, :]
    sine = jnp.sin(angles)
    return jnp.cos(angles), jnp.where(lanes[None, :] < half_width, -sine, sine)


def local(
    dims,
    query_latent, joint_latent, rotary_key, query_gain, joint_gain, query_weight, query_rotary,
    key_weight, value_weight, output_weight, expert_input, expert_gain, routes, route_weight,
    gate_weight, up_weight, down_weight,
):
    ny, nx, nz = dims
    ep_n, tokens, width = ny * nx, query_latent.shape[0], output_weight.shape[1]
    cap = 3 * tokens // (2 * ep_n)
    rows = ep_n * cap
    half = tokens // 2
    cos, sin = rotary_tables(tokens)

    hz = nz // 2
    per = tokens // (2 * nz)
    sds = jax.ShapeDtypeStruct
    vmem = pl.BlockSpec(memory_space=pltpu.VMEM)
    hbm = pl.BlockSpec(memory_space=pl.ANY)
    sem = pltpu.SemaphoreType.DMA
    side = max(ny, nx)
    streamed = [
        expert_input, joint_latent, key_weight, value_weight, query_latent, query_weight, query_rotary.T,
        gate_weight, up_weight, down_weight, output_weight,
    ]
    scratch = [pltpu.VMEM(a.shape, a.dtype) for a in streamed] + [
        pltpu.VMEM((2, ep_n, hz, cap, LANES), BF16),
        pltpu.VMEM((2, hz, 2, 2, rows, LANES), BF16),
        pltpu.VMEM((2, nz, 2, rows, LANES), BF16),
        pltpu.VMEM((2, nz, rows, LANES), BF16),
        pltpu.VMEM((2, 2, hz, rows, LANES), BF16),
        pltpu.VMEM((2, 2, hz, rows, LANES), BF16),
        pltpu.VMEM((2, rows, LANES), BF16),
        pltpu.VMEM((2 * ep_n, cap, LANES), BF16),
        pltpu.VMEM((2, side, side, LANES + ROPE, half), BF16),
        pltpu.VMEM((2, side, side, half, LANES), BF16),
        pltpu.VMEM((2, tokens, LANES), BF16),
        pltpu.VMEM((tokens, 8), F32),
        pltpu.VMEM((2, tokens, LANES), F32),
        pltpu.VMEM((2, tokens, LANES), F32),
        pltpu.VMEM((2, tokens, LANES), F32),
        pltpu.VMEM((nz, 2, per, width), BF16),
        pltpu.VMEM((nz, per, width), BF16),
        pltpu.VMEM((2, hz, per, width), BF16),
        pltpu.VMEM((2, hz, per, width), BF16),
        sem((2, 2, ep_n)), sem((2, 2, ep_n)),
        sem((2, hz)), sem((2, hz)),
        sem((2, hz + 2)), sem((2, hz + 2)),
        sem((2, 8, 2, 2, 2)), sem((2, 8, 2, 2, 2)),
        sem((2, 4)), sem((2, 4)),
        sem((2, 2, 2, hz)), sem((2, 2, 2, hz)),
        sem((2, ep_n)), sem((2, ep_n)),
        sem((2,)), sem((2,)),
        sem((2, 2, hz)), sem((2, 2, hz)),
        sem((len(streamed),)),
        sem((2,)),
    ]
    mixer, expert = pl.pallas_call(
        functools.partial(main_kernel, (ny, nx, nz, cap)),
        out_shape=(sds((per, width), BF16), sds((tokens, LANES), BF16)),
        in_specs=[vmem] * 8 + [hbm] * len(streamed),
        out_specs=(vmem, vmem),
        scratch_shapes=scratch,
        compiler_params=pltpu.CompilerParams(
            collective_id=0, has_side_effects=True, vmem_limit_bytes=62 * 2**20
        ),
        name="main",
    )(
        routes.T, route_weight.T, query_gain[None], joint_gain[None], expert_gain[None], rotary_key.T, cos, sin,
        *streamed,
    )
    return pl.pallas_call(
        back_kernel,
        out_shape=(sds(mixer.shape, BF16), sds(expert.shape, BF16)),
        name="back",
    )(mixer, expert)


def solution(mesh):
    ny, nx = ep_grid(mesh.shape["ep"])
    return jax.shard_map(
        functools.partial(local, (ny, nx, mesh.shape["tp"] // 2)),
        mesh=mesh,
        in_specs=(
            P("ep", None),
            P("ep", None),
            P("ep", None),
            P(),
            P(),
            P(None, "tp"),
            P(None, "tp"),
            P(None, "tp"),
            P(None, "tp"),
            P("tp", None),
            P("ep", None),
            P(),
            P("ep", None),
            P("ep", None),
            P("ep", None, "tp"),
            P("ep", None, "tp"),
            P("ep", "tp", None),
        ),
        out_specs=(P(("ep", "tp"), None), P("ep", "tp")),
        check_vma=False,
    )
```

time: 141 us -> 98.6 us (0.70); the launches traced: 139 us -> 98.5 us
  Pallas kernels: 120 us -> 96 us
  local copies, waits for them, and re-layouts: 15.8 us -> 0 us
    pallas_call x1, Pallas kernels: 114 us -> 94.3 us  [local(): pl.pallas_call(functools.partial(main_kernel, (ny, nx, nz, cap)), out_sha...]
    concatenate x4 -> x0, local copies, waits for them, and re-layouts: 7.72 us -> none  [placed(): return jnp.concatenate([plain0, rope0, pad, pad, rope1, plain1], axis=1)]
    unnamed x19 -> x0, local copies, waits for them, and re-layouts: 5.98 us -> none
    pallas_call x1, Pallas kernels: 6.02 us -> 1.68 us  [local(): pl.pallas_call(back_kernel, out_shape=(sds(mixer.shape, BF16), sds(expert...]
    select_n x0 -> x1, other arithmetic: none -> 1.83 us  [rotary_tables(): jnp.where(lanes[None, :] < half_width, -sine, sine)]
    slice x8 -> x0, local copies, waits for them, and re-layouts: 1.78 us -> none  [the longest x5 1.51 us: swapped(): return jnp.concatenate([w[:, hw:], w[:, :hw]], axis=1)]
where the time goes in v2:
time: 98.6 us; the launch traced here: 98.5 us
  Pallas kernels  96 us (97%)
  other arithmetic  1.85 us (2%)
    pallas_call x1, Pallas kernels, local(): pl.pallas_call(functools.partial(main_kernel, (ny, nx, nz, cap)), out_sha...  94.3 us

profile of v2, /device:TPU:1, one launch (start us, length us, event | category | flops | bytes accessed | tf_op | source)
XLA Modules:
  0.0 98.5 jit_solution(17977076919605523202)
XLA Ops:
  0.7 1.8 %negate_select_fusion = (f32[512,128]{1,0:T(8,128)}, f32[512,128]{1,0:T(8,128)}) fusion(f32[128]{0:T(128)S(1)} %fusion.3, f32[512]{0:T(512)S(1)} %add_convert_fusion, pred[128]{0:T(512)(128)(4,1)S(1)} %broadcast_compare_fusion), kind=kLoop, calls=%fused_computation | loop fusion | flops 196608 | bytes 526976 | tf_op jit(solution)/shard_map/jit(_where)/select_n | solution.py:566
  2.5 94.3 %main.1 = (bf16[32,2048]{1,0:T(8,128)(2,1)}, bf16[512,128]{1,0:T(8,128)(2,1)}) custom-call(s32[2,512]{1,0:T(2,128)} %bitcast.10, f32[2,512]{1,0:T(2,128)} %bitcast.11, f32[1,1024]{1,0:T(1,128)} %bitcast.12, f32[1,512]{1,0:T(1,128)} %bitcast.13, f32[1,2048]{1,0:T(1,128)} %bitcast.9, bf16[32,512]{1,0:T(8,128)(2,1)} %bitcast.8, ...), custom_call_target="tpu_custom_call" | custom-call | tf_op jit(solution)/shard_map/main/pallas_call | solution.py:625
  96.8 1.7 %back.1 = (bf16[32,2048]{1,0:T(8,128)(2,1)}, bf16[512,128]{1,0:T(8,128)(2,1)}) custom-call(bf16[32,2048]{1,0:T(8,128)(2,1)} %get-tuple-element.4.mixer, bf16[512,128]{1,0:T(8,128)(2,1)} %get-tuple-element.5.expert), custom_call_target="tpu_custom_call" | custom-call | tf_op jit(solution)/shard_map/back/pallas_call | solution.py:639
  (3 shorter events, 0.0 us)

commit v3 on v2

--- a/solution.py
+++ b/solution.py
@@ -68,6 +68,11 @@
         d.start()
         pending.append(d)
 
+    def flush(count):
+        with jax.named_scope(f"flush#n={count}"):
+            for _ in range(min(count, len(pending))):
+                pending.pop(0).wait_send()
+
     def arrived(dst, ssem, rsem, frm):
         pltpu.make_async_remote_copy(
             src_ref=dst, dst_ref=dst, send_sem=ssem, recv_sem=rsem, device_id=frm, device_id_type=MESH
@@ -102,7 +107,7 @@
         named = named0 | named1
         before = dot(named.astype(F32).astype(BF16), (row < col).astype(F32).astype(BF16))
         rank = jnp.where(named, before, -1.0)
-        place = before + (sub_e * cap).astype(F32)
+        place = before + ((lax.rem(sub_e, 2) * ep_n + sub_e // 2) * cap).astype(F32)
         slot0 = jnp.sum(jnp.where(named0, place, 0.0), axis=0, keepdims=True)
         slot1 = jnp.sum(jnp.where(named1, place, 0.0), axis=0, keepdims=True)
         stack = jnp.concatenate([slot0, slot1, rw_ref[...], jnp.zeros((4, tokens), F32)], axis=0)
@@ -142,7 +147,10 @@
             for k in range(1, ep_n):
                 to = lax.rem(ep + k, ep_n)
                 there = xbuf.at[e, span, par, c, mine_rows]
-                send(slots.at[e, to, span], there, a2a_s.at[e, g, k], a2a_r.at[e, g, k], (to, tp))
+                pltpu.make_async_remote_copy(
+                    src_ref=slots.at[e, to, span], dst_ref=there, send_sem=a2a_s.at[e, g], recv_sem=a2a_r.at[e, g],
+                    device_id=(to, tp), device_id_type=MESH,
+                ).start()
         pltpu.make_async_copy(slots.at[e, ep], xbuf.at[e, :, par, c, mine_rows], own_s.at[e]).start()
 
     axes = (("x", nx, x), ("y", ny, y))
@@ -248,10 +256,12 @@
         with jax.named_scope(f"a2a_wait#e={e}#g={g}"):
             if g == 0:
                 pltpu.make_async_copy(slots.at[e, ep], xbuf.at[e, :, par, c, mine_rows], own_s.at[e]).wait()
-            for k in range(1, ep_n):
-                frm = lax.rem(ep + ep_n - k, ep_n)
-                there = xbuf.at[e, span, par, c, pl.ds(pl.multiple_of(frm * cap, 16), cap)]
-                arrived(there, a2a_s.at[e, g, k], a2a_r.at[e, g, k], (frm, tp))
+            both = pltpu.make_async_remote_copy(
+                src_ref=slots.at[e, pl.ds(0, ep_n - 1), span], dst_ref=xbuf.at[e, span, par, c, pl.ds(0, rows - cap)],
+                send_sem=a2a_s.at[e, g], recv_sem=a2a_r.at[e, g], device_id=sib, device_id_type=MESH,
+            )
+            both.wait_recv()
+            pending.append(both)
         for i in members[g]:
             piece = xbuf.at[e, i, par, c]
             send(piece, piece, zs.at[e, i], zr.at[e, i], z_to[i % 2])
@@ -368,8 +378,11 @@
             for k in range(1, ep_n):
                 to = lax.rem(ep + k, ep_n)
                 src = fin.at[e, pl.ds(pl.multiple_of(to * cap, 16), cap)]
-                send(src, ret.at[2 * ep + e], bks.at[e, k], bkr.at[e, k], (to, tp))
-            ret[2 * ep + e] = fin[e, mine_rows]
+                pltpu.make_async_remote_copy(
+                    src_ref=src, dst_ref=ret.at[e, ep], send_sem=bks.at[e], recv_sem=bkr.at[e],
+                    device_id=(to, tp), device_id_type=MESH,
+                ).start()
+            ret[e, ep] = fin[e, mine_rows]
 
     q_tile = min(256, tokens)
 
@@ -440,9 +453,12 @@
     def combine():
         with jax.named_scope("combine_wait"):
             for e in (0, 1):
-                for k in range(1, ep_n):
-                    frm = lax.rem(ep + ep_n - k, ep_n)
-                    arrived(ret.at[2 * frm + e], bks.at[e, k], bkr.at[e, k], (frm, tp))
+                both = pltpu.make_async_remote_copy(
+                    src_ref=fin.at[e, pl.ds(0, rows - cap)], dst_ref=ret.at[e, pl.ds(0, ep_n - 1)],
+                    send_sem=bks.at[e], recv_sem=bkr.at[e], device_id=sib, device_id_type=MESH,
+                )
+                both.wait_recv()
+                pending.append(both)
         with jax.named_scope("combine"):
             slot_count = experts * cap
             where_at = lax.broadcasted_iota(jnp.int32, (tokens, slot_count), 1).astype(F32)
@@ -492,10 +508,10 @@
     queries()
     a2a_wait(0, 0)
     a2a_wait(0, 1)
+    z_wait(0, 0)
     a2a_wait(1, 0)
-    z_wait(0, 0)
+    z_wait(0, 1)
     a2a_wait(1, 1)
-    z_wait(0, 1)
     for name in ("wg", "wu", "wd"):
         loads[name].wait()
     expert(0)
@@ -508,47 +524,53 @@
     step_of(0)
     pair(1)
     red[1][0]()
-    step_of(0)
     kv_line(2)
     work(1)
     step_of(0)
-    work(1)
+    work(3)
+    step_of(0)
+    flush(60)
+    step_of(1)
+    kv_upto(1)
+    kv_upto(2)
+    work(2)
+    step_of(1)
+    work(3)
+    step_of(0)
+    work(2)
     step_of(0)
     work(2)
     step_of(1)
-    kv_upto(1)
-    step_of(1)
-    step_of(0)
-    kv_upto(2)
-    work(2)
-    for e in (0, 1, 1, 0):
-        step_of(e)
-        work(2)
-    step_of(1)
-    kv_upto(3)
     work(len(todo))
     out_proj()
+    step_of(1)
     step_of(0)
     with jax.named_scope("pair#a"):
         for q in range(0, nz, hz):
             arrived(asb.at[pl.ds(q, hz)], aps.at[q // hz], apr.at[q // hz], sib)
     red[2][0]()
-    for e in (1, 2, 1, 2, 1, 2, 2):
-        step_of(e)
+    step_of(0)
+    flush(50)
+    step_of(1)
+    step_of(1)
+    step_of(2)
+    step_of(2)
+    step_of(1)
     for e in (0, 1):
         while red[e][3]:
             step_of(e)
-    while len(red[2][3]) > 1:
+    flush(40)
+    for _ in range(3):
         step_of(2)
     combine()
+    flush(len(pending) - 2)
     while red[2][3]:
         step_of(2)
     cut = mixer_ref.shape[0] // 2
     for g, v in enumerate(red[2][2]()):
         mixer_ref[g * cut : (g + 1) * cut] = v
 
-    for d in pending:
-        d.wait_send()
+    flush(len(pending))
 
 
 def back_kernel(mixer, expert, mixer_out, expert_out):
@@ -598,7 +620,7 @@
         pltpu.VMEM((2, 2, hz, rows, LANES), BF16),
         pltpu.VMEM((2, 2, hz, rows, LANES), BF16),
         pltpu.VMEM((2, rows, LANES), BF16),
-        pltpu.VMEM((2 * ep_n, cap, LANES), BF16),
+        pltpu.VMEM((2, ep_n, cap, LANES), BF16),
         pltpu.VMEM((2, side, side, LANES + ROPE, half), BF16),
         pltpu.VMEM((2, side, side, half, LANES), BF16),
         pltpu.VMEM((2, tokens, LANES), BF16),
@@ -610,13 +632,13 @@
         pltpu.VMEM((nz, per, width), BF16),
         pltpu.VMEM((2, hz, per, width), BF16),
         pltpu.VMEM((2, hz, per, width), BF16),
-        sem((2, 2, ep_n)), sem((2, 2, ep_n)),
+        sem((2, 2)), sem((2, 2)),
         sem((2, hz)), sem((2, hz)),
         sem((2, hz + 2)), sem((2, hz + 2)),
         sem((2, 8, 2, 2, 2)), sem((2, 8, 2, 2, 2)),
         sem((2, 4)), sem((2, 4)),
         sem((2, 2, 2, hz)), sem((2, 2, 2, hz)),
-        sem((2, ep_n)), sem((2, ep_n)),
+        sem((2,)), sem((2,)),
         sem((2,)), sem((2,)),
         sem((2, 2, hz)), sem((2, 2, hz)),
         sem((len(streamed),)),

time: 98.6 us -> 91.5 us (0.928)
  Pallas kernels: 96 us -> 88.9 us
    pallas_call x1, Pallas kernels: 94.3 us -> 87.2 us  [local(): pl.pallas_call(functools.partial(main_kernel, (ny, nx, nz, cap)), out_sha...]
where the time goes in v3:
time: 91.5 us; the launch traced here: 91.4 us
  Pallas kernels  88.9 us (97%)
  other arithmetic  1.85 us (2%)
    pallas_call x1, Pallas kernels, local(): pl.pallas_call(functools.partial(main_kernel, (ny, nx, nz, cap)), out_sha...  87.2 us
    select_n x1, other arithmetic, rotary_tables(): jnp.where(lanes[None, :] < half_width, -sine, sine)  1.83 us

profile of v3, /device:TPU:1, one launch (start us, length us, event | category | flops | bytes accessed | tf_op | source)
XLA Modules:
  0.0 91.4 jit_solution(12856247228881285400)
XLA Ops:
  0.7 1.8 %negate_select_fusion = (f32[512,128]{1,0:T(8,128)}, f32[512,128]{1,0:T(8,128)}) fusion(f32[128]{0:T(128)S(1)} %fusion.3, f32[512]{0:T(512)S(1)} %add_convert_fusion, pred[128]{0:T(512)(128)(4,1)S(1)} %broadcast_compare_fusion), kind=kLoop, calls=%fused_computation | loop fusion | flops 196608 | bytes 526976 | tf_op jit(solution)/shard_map/jit(_where)/select_n | solution.py:588
  2.5 87.2 %main.1 = (bf16[32,2048]{1,0:T(8,128)(2,1)}, bf16[512,128]{1,0:T(8,128)(2,1)}) custom-call(s32[2,512]{1,0:T(2,128)} %bitcast.10, f32[2,512]{1,0:T(2,128)} %bitcast.11, f32[1,1024]{1,0:T(1,128)} %bitcast.12, f32[1,512]{1,0:T(1,128)} %bitcast.13, f32[1,2048]{1,0:T(1,128)} %bitcast.9, bf16[32,512]{1,0:T(8,128)(2,1)} %bitcast.8, ...), custom_call_target="tpu_custom_call" | custom-call | tf_op jit(solution)/shard_map/main/pallas_call | solution.py:647
  89.7 1.7 %back.1 = (bf16[32,2048]{1,0:T(8,128)(2,1)}, bf16[512,128]{1,0:T(8,128)(2,1)}) custom-call(bf16[32,2048]{1,0:T(8,128)(2,1)} %get-tuple-element.4.mixer, bf16[512,128]{1,0:T(8,128)(2,1)} %get-tuple-element.5.expert), custom_call_target="tpu_custom_call" | custom-call | tf_op jit(solution)/shard_map/back/pallas_call | solution.py:661
  (3 shorter events, 0.0 us)
